TPU v7x, 512 devices: a whole 4x8x8 slice. The times are simulated.
512 devices in a mesh: sp: 32 (over z, x), tp: 16 (over y, core).
Axes of the slice: x: 4, y: 8, z: 8, core: 2. Of those that a mesh axis runs over, the one named last changes fastest.
Arguments:
- mixer_out: bfloat16 [4096, 2048], P('sp'), may hold values from -6 to 6
- out_grad: bfloat16 [4096, 2048], P('sp'), may hold values from -2 to 2
- route_ids: int32 [4096, 2], P('sp'), may hold values from 0 to 31, all different within a row; in each aligned block of 128 rows (0 to 127, 128 to 255, ...) at most 16 rows name the same one
- route_weights: float32 [4096, 2], P('sp'), may hold values from 0.2 to 1.2
- gate_branch: bfloat16 [4096, 2048], P('sp', 'tp'), may hold values from -4 to 4
- states: float32 [4096, 2048], P('sp', 'tp'), may hold values from -6 to 6
- decay: float32 [4096, 2048], P('sp', 'tp'), may hold values from 0 to 1
- w_proj: bfloat16 [2048, 2048], P(None, 'tp'), may hold values from -0.125 to 0.125
- w_gate: bfloat16 [32, 2048, 2048], P('sp', 'tp'), may hold values from -0.125 to 0.125
- w_up: bfloat16 [32, 2048, 2048], P('sp', 'tp'), may hold values from -0.125 to 0.125
- w_down: bfloat16 [32, 2048, 2048], P('sp', 'tp'), may hold values from -0.125 to 0.125
Outputs:
- grad_w_gate: bfloat16 [32, 2048, 2048], P('sp', 'tp')
- grad_w_up: bfloat16 [32, 2048, 2048], P('sp', 'tp')
- grad_w_down: bfloat16 [32, 2048, 2048], P('sp', 'tp')
- grad_w_proj: float32 [2048, 2048], P('sp', 'tp')
- grad_branch: bfloat16 [4096, 2048], P('sp', 'tp')
- grad_drive: float32 [4096, 2048], P('sp', 'tp')
- grad_decay: float32 [4096, 2048], P('sp', 'tp')
Inputs may be any that keep to these rules, and one draw needn't show every extreme that they name: `route_ids`: each row names 2 different experts. In the rows of one index of sp no expert is named more than 16 times, a bound that some block reaches.
All inputs are finite; a program needn't handle non-finite values.
Results may differ from a plain program's by a relative error of at most 0.02.
Values may be sent and summed in bfloat16 or wider, within the bound.
A program may use at most 64 MiB of HBM per device.

v0:
```python
import jax
import jax.numpy as jnp
from jax import lax
from jax.sharding import PartitionSpec as P


def in_one_piece(arrays, axis, split_dim, concat_dim, along):
    widths = [a.shape[along] for a in arrays]
    both = jnp.concatenate(arrays, axis=along)
    result = lax.all_to_all(both, axis, split_axis=split_dim, concat_axis=concat_dim, tiled=True)
    return tuple(jnp.split(result, [sum(widths[:k]) for k in range(1, len(widths))], axis=along))


def sent_together(arrays, axis, dim, along):
    widths = [a.shape[along] for a in arrays]
    both = jnp.concatenate(arrays, axis=along)
    result = lax.all_gather(both, axis, axis=dim, tiled=True)
    return tuple(jnp.split(result, [sum(widths[:k]) for k in range(1, len(widths))], axis=along))


def gathered_total(shard, axis):
    return lax.all_gather(shard, axis).astype(jnp.float32).sum(0)


def in_blocks(shard, dim, length):
    before, after = (shard.shape[:dim], shard.shape[dim + 1 :])
    return jnp.moveaxis(shard.reshape(*before, length, -1, *after), dim, 0)


def sum_at_owner(shard, axis, dim):
    pieces = in_blocks(shard, dim, lax.axis_size(axis))
    arrived = lax.all_to_all(pieces, axis, split_axis=0, concat_axis=0, tiled=True)
    return arrived.astype(jnp.float32).sum(axis=0)


def copy_for_each(shard, axis):
    copies = jnp.broadcast_to(shard, (lax.axis_size(axis), *shard.shape))
    return lax.all_to_all(copies, axis, split_axis=0, concat_axis=0, tiled=True)


def gathered_once(shard, axis):
    leaves = jax.tree.leaves(shard)
    sequence = sorted(range(len(leaves)), key=lambda k: -leaves[k].size)
    width = (1, *leaves[sequence[0]].shape)[-1]
    lines = [
        jnp.pad(leaves[k].reshape(-1), (0, -leaves[k].size % width)).reshape(-1, width)
        for k in sequence
    ]
    both, at, found = (copy_for_each(jnp.concatenate(lines), axis), 0, {})
    for k, line in zip(sequence, lines):
        slab = both[:, at : at + len(line)].reshape(len(both), -1)
        found[k] = slab[:, : leaves[k].size].reshape(-1, *leaves[k].shape)
        at += len(line)
    numbers = iter(range(len(leaves)))
    return jax.tree.map(lambda _: found[next(numbers)], shard)


def folded_in_pairs(pieces, combine):
    while len(jax.tree.leaves(pieces)[0]) > 1:
        pieces = jax.vmap(combine)(
            *(jax.tree.map(lambda part: part[side::2], pieces) for side in (0, 1))
        )
    return jax.tree.map(lambda part: part[0], pieces)


def entering(shard, axis, combine, identity):
    length, position = (lax.axis_size(axis), lax.axis_index(axis))
    passed = jnp.arange(length) > position

    def kept(part, zero, own):
        part = jnp.where(
            passed.reshape(-1, *(1 for _ in own.shape)), part, jnp.asarray(zero, own.dtype)
        )
        return part[::-1]

    pieces = gathered_once(shard, axis)
    return folded_in_pairs(jax.tree.map(kept, pieces, identity, shard), combine)


def shifted(block, axis, distance):
    devices = range(lax.axis_size(axis))
    route = [(i - distance, i) for i in devices if i - distance in devices]
    return lax.ppermute(block, axis, route)


def linear_combine(earlier, later):
    return (earlier[0] * later[0], later[0] * earlier[1] + later[1])


def chain_combine(earlier, later):
    return (later[0] * earlier[0], later[1] + later[0] * earlier[1])


def expert_grads(inputs, cotangents, w_gate, w_up, w_down):
    gate_pre = jnp.einsum("esd,efd->esf", inputs, w_gate, preferred_element_type=jnp.float32)
    up_pre = jnp.einsum("esd,efd->esf", inputs, w_up, preferred_element_type=jnp.float32)
    sigmoid_gate = jax.nn.sigmoid(gate_pre)
    silu_gate = gate_pre * sigmoid_gate
    hidden = (silu_gate * up_pre).astype(jnp.bfloat16)
    hidden_grad = jnp.einsum("esd,efd->esf", cotangents, w_down, preferred_element_type=jnp.float32)
    up_grad = (hidden_grad * silu_gate).astype(jnp.bfloat16)
    gate_grad = (
        hidden_grad * up_pre * sigmoid_gate * (1.0 + gate_pre * (1.0 - sigmoid_gate))
    ).astype(jnp.bfloat16)
    grad_gate = jnp.einsum(
        "esf,esd->efd", gate_grad, inputs, preferred_element_type=jnp.float32
    ).astype(jnp.bfloat16)
    grad_up = jnp.einsum(
        "esf,esd->efd", up_grad, inputs, preferred_element_type=jnp.float32
    ).astype(jnp.bfloat16)
    grad_down = jnp.einsum(
        "esf,esd->efd", hidden, cotangents, preferred_element_type=jnp.float32
    ).astype(jnp.bfloat16)
    partial_value = jnp.einsum(
        "esf,efd->esd", gate_grad, w_gate, preferred_element_type=jnp.float32
    )
    partial_value = partial_value + jnp.einsum(
        "esf,efd->esd", up_grad, w_up, preferred_element_type=jnp.float32
    )
    return (grad_gate, grad_up, grad_down, partial_value.astype(jnp.bfloat16))


def local(
    mixer_out,
    out_grad,
    route_ids,
    route_weights,
    gate_branch,
    states,
    decay,
    w_proj,
    w_gate,
    w_up,
    w_down,
):
    tok_rows, model_width = mixer_out.shape
    top_count = route_ids.shape[1]
    local_experts = w_gate.shape[0]
    sp_size = lax.axis_size("sp")
    tp_size = lax.axis_size("tp")
    experts = local_experts * sp_size
    capacity = 2 * top_count * tok_rows // experts
    routes = tok_rows * top_count
    flat_ids = route_ids.reshape(-1)
    onehot = (flat_ids[:, None] == jnp.arange(experts, dtype=jnp.int32)[None, :]).astype(jnp.int32)
    position = jnp.sum(jnp.cumsum(onehot, axis=0) * onehot, axis=1) - 1
    bucket = flat_ids % local_experts * sp_size + flat_ids // local_experts
    slot_index = bucket * capacity + position
    source = (
        jnp.full((experts * capacity,), routes, jnp.int32)
        .at[slot_index]
        .set(jnp.arange(routes, dtype=jnp.int32))
    )
    scaled = (route_weights[:, :, None] * out_grad[:, None, :].astype(jnp.float32)).astype(
        jnp.bfloat16
    )
    scaled_pad = jnp.concatenate(
        [scaled.reshape(routes, model_width), jnp.zeros((1, model_width), jnp.bfloat16)], axis=0
    )
    token_pad = jnp.concatenate([mixer_out, jnp.zeros((1, model_width), jnp.bfloat16)], axis=0)
    slot_shape = (local_experts, sp_size, capacity, model_width)
    x_send = token_pad[source // top_count].reshape(slot_shape)
    c_send = scaled_pad[source].reshape(slot_shape)
    slot_share = capacity // tp_size
    first_slot = lax.axis_index("tp") * slot_share
    x_part = lax.dynamic_slice_in_dim(x_send, first_slot, slot_share, 2)
    c_part = lax.dynamic_slice_in_dim(c_send, first_slot, slot_share, 2)
    x_part, c_part = in_one_piece((x_part, c_part), "sp", 1, 1, 0)
    x_recv, c_recv = sent_together((x_part, c_part), "tp", 2, 0)
    grad_gate, grad_up, grad_down, partial_value = expert_grads(
        x_recv.reshape(local_experts, -1, model_width),
        c_recv.reshape(local_experts, -1, model_width),
        w_gate,
        w_up,
        w_down,
    )
    pieces = lax.all_to_all(
        partial_value.reshape(slot_shape), "tp", split_axis=2, concat_axis=0, tiled=True
    )
    summed = jnp.sum(
        pieces.reshape(tp_size, local_experts, sp_size, slot_share, model_width).astype(
            jnp.float32
        ),
        axis=0,
    )
    returned = lax.all_to_all(
        summed.astype(jnp.bfloat16), "sp", split_axis=1, concat_axis=1, tiled=True
    ).astype(summed.dtype)
    offset = position - first_slot
    inside = ((offset >= 0) & (offset < slot_share)).astype(jnp.float32)
    index_part = bucket * slot_share + jnp.clip(offset, 0, slot_share - 1)
    picked = returned.reshape(-1, model_width)[index_part] * inside[:, None]
    token_part = jnp.sum(picked.reshape(tok_rows, top_count, model_width), axis=1)
    routed_total = gathered_total(token_part.astype(jnp.bfloat16), "tp").astype(jnp.float32)
    mid_grad = (out_grad.astype(jnp.float32) + routed_total).astype(jnp.bfloat16)
    gated = (gate_branch.astype(jnp.float32) * states).astype(jnp.bfloat16)
    proj_grad = sum_at_owner(
        lax.dot_general(
            mid_grad, gated, (((0,), (0,)), ((), ())), preferred_element_type=jnp.float32
        ).astype(jnp.bfloat16),
        "sp",
        0,
    )
    act_grad = jnp.dot(mid_grad, w_proj, preferred_element_type=jnp.float32)
    branch_grad = (act_grad * states).astype(jnp.bfloat16)
    state_grad = act_grad * gate_branch.astype(jnp.float32)
    channels = decay.shape[1]
    next_decay = jnp.concatenate([decay[1:], jnp.ones((1, channels), jnp.float32)], axis=0)
    decay_prod, local_grad = lax.associative_scan(
        linear_combine, (next_decay[::-1], state_grad[::-1]), axis=0
    )
    decay_prod = decay_prod[::-1]
    local_grad = local_grad[::-1]
    head_decay = decay[0]
    carried = entering(
        (head_decay * decay_prod[0], head_decay * local_grad[0]),
        "sp",
        chain_combine,
        (jnp.ones_like(head_decay), jnp.zeros_like(head_decay)),
    )
    drive_grad = local_grad + decay_prod * carried[1][None, :]
    before = shifted(states[-1:], "sp", 1)
    previous = jnp.concatenate([before, states[:-1]], axis=0)
    decay_grad = drive_grad * previous
    return (grad_gate, grad_up, grad_down, proj_grad, branch_grad, drive_grad, decay_grad)


def solution(mesh):
    placed = (
        P("sp", None),
        P("sp", None),
        P("sp", None),
        P("sp", None),
        P("sp", "tp"),
        P("sp", "tp"),
        P("sp", "tp"),
        P(None, "tp"),
        P("sp", "tp", None),
        P("sp", "tp", None),
        P("sp", "tp", None),
    )
    return jax.shard_map(
        local,
        mesh=mesh,
        in_specs=placed,
        out_specs=(
            P("sp", "tp", None),
            P("sp", "tp", None),
            P("sp", "tp", None),
            P("sp", "tp"),
            P("sp", "tp"),
            P("sp", "tp"),
            P("sp", "tp"),
        ),
        check_vma=False,
    )
```

profile of v0, /device:TPU:1, one launch (start us, length us, event | category | flops | bytes accessed | tf_op | source)
XLA Modules:
  0.0 301.0 jit_solution(11442101873857682081)
XLA Ops:
  8.5 2.1 mul.215
  10.6 2.4 mul.216
  14.3 1.4 scatter_custom_fusion
  15.7 1.8 multiply_convert_fusion
  17.7 3.3 %gather_fusion.1 = bf16[512,2048]{1,0:T(8,128)(2,1)} fusion(bf16[257,2048]{1,0:T(8,128)(2,1)S(1)} %concatenate.56, s32[1024]{0:T(1024)S(1)} %get-tuple-element.63), kind=kCustom, calls=%fused_computation.1 | custom fusion | bytes 4196352 | tf_op jit(solution)/shard_map/gather | solution.py:163
  21.0 1.5 dynamic-slice_bitcast_fusion
  22.5 2.5 gather_fusion
  25.9 24.8 %all_to_all.29 = bf16[2,32,1,2048]{3,0,2,1:T(2,128)(2,1)S(1)} all-to-all(bf16[2,32,1,2048]{3,0,2,1:T(2,128)(2,1)S(1)} %pad_maximum_fusion), channel_id=1, replica_groups=mesh['sp'=32,'tp'=16] {'sp'}, dimensions={1} | all-to-all | bytes 524288 | tf_op jit(solution)/shard_map/all_to_all | solution.py:10
  51.5 42.2 %all-gather.4.cloned.1.call-done = bf16[2,32,16,2048]{3,1,0,2:T(8,128)(2,1)} async-done(((bf16[2,32,1,2048]{3,1,0,2:T(8,128)(2,1)}), bf16[2,32,16,2048]{3,1,0,2:T(8,128)(2,1)}) %all-gather.4.cloned.1.call-update) | async-done | bytes 4194320 | tf_op jit(solution)/shard_map/all_gather | solution.py:17
  93.7 2.7 fusion.28
  96.4 1.2 copy.65
  99.3 1.2 copy.64
  103.3 1.2 copy.58
  104.5 55.3 %all_to_all.30 = bf16[1,32,16,2048]{3,1,0,2:T(8,128)(2,1)} all-to-all(bf16[1,32,16,2048]{3,1,0,2:T(8,128)(2,1)S(1)} %copy.58), channel_id=1, replica_groups=mesh['sp'=32,'tp'=16] {'tp'}, dimensions={2} | all-to-all | bytes 4194304 | tf_op jit(solution)/shard_map/all_to_all | solution.py:177
  159.7 2.0 reduce_sum.51
  162.4 1.4 reduce.7
  164.5 9.9 %all-to-all-start.2 = ((bf16[32,2,1024]{2,1,0:T(2,128)(2,1)}), bf16[32,2,1024]{2,1,0:T(2,128)(2,1)S(1)}, u32[]{:S(2)}, u32[]{:S(2)}) async-start(bf16[32,2,1024]{2,1,0:T(2,128)(2,1)} %reshape.296), calls=%async_computation.2 | async-start | bytes 262144 | tf_op jit(solution)/shard_map/all_to_all | solution.py:186
  175.5 9.3 %all-to-all-done.2 = bf16[32,2,1024]{2,1,0:T(2,128)(2,1)S(1)} async-done(((bf16[32,2,1024]{2,1,0:T(2,128)(2,1)}), bf16[32,2,1024]{2,1,0:T(2,128)(2,1)S(1)}, u32[]{:S(2)}, u32[]{:S(2)}) %all-to-all-start.2) | async-done | bytes 131104 | tf_op jit(solution)/shard_map/all_to_all | solution.py:186
  185.0 2.7 gather_fusion.2
  187.7 3.5 %gather.14 = f32[128,2,2048]{2,1,0:T(2,128)} reshape(f32[256,2048]{1,0:T(8,128)} %gather_fusion.2) | data formatting | bytes 4194304 | tf_op jit(solution)/shard_map/gather | solution.py:192
  191.2 5.6 %multiply_reduce_fusion = bf16[128,2048]{1,0:T(8,128)(2,1)} fusion(f32[128,2,2048]{2,1,0:T(2,128)} %gather.14, f32[128,2]{1,0:T(8,128)S(1)} %copy-done.12), kind=kLoop, calls=%fused_computation.13 | loop fusion | flops 786432 | bytes 2622464 | tf_op jit(solution)/shard_map/reduce_sum | solution.py:193
  196.9 1.3 collective-permute-start
  198.9 1.3 fusion
  200.2 1.3 fusion.1
  201.5 1.3 fusion.2
  202.8 43.6 %all-gather.6.cloned.1.call-done = bf16[2048,2048]{1,0:T(8,128)(2,1)} async-done(((bf16[128,2048]{1,0:T(8,128)(2,1)}), bf16[2048,2048]{1,0:T(8,128)(2,1)}) %all-gather.6.cloned.1.call-update) | async-done | bytes 8388624 | tf_op jit(solution)/shard_map/all_gather | solution.py:22
  246.4 5.4 %convert_reduce_fusion = f32[128,2048]{1,0:T(8,128)S(1)} fusion(bf16[16,128,2048]{2,1,0:T(8,128)(2,1)} %bitcast.81), kind=kLoop, calls=%fused_computation.4 | loop fusion | flops 8126464 | bytes 9437184 | tf_op jit(solution)/shard_map/reduce_sum | solution.py:22
  255.6 9.9 %all-to-all-start.4 = ((f32[32,2,128]{2,1,0:T(2,128)}), f32[32,2,128]{2,1,0:T(2,128)S(1)}, u32[]{:S(2)}, u32[]{:S(2)}) async-start(f32[32,2,128]{2,1,0:T(2,128)} %broadcast_in_dim.43), calls=%async_computation.4 | async-start | bytes 65536 | tf_op jit(solution)/shard_map/all_to_all | solution.py:38
  265.5 1.2 convolution_convert_fusion
  266.7 7.5 %all-to-all-done.4 = f32[32,2,128]{2,1,0:T(2,128)S(1)} async-done(((f32[32,2,128]{2,1,0:T(2,128)}), f32[32,2,128]{2,1,0:T(2,128)S(1)}, u32[]{:S(2)}, u32[]{:S(2)}) %all-to-all-start.4) | async-done | bytes 32800 | tf_op jit(solution)/shard_map/all_to_all | solution.py:38
  274.2 3.9 %all-to-all-start.3 = ((bf16[32,64,128]{2,1,0:T(8,128)(2,1)}), bf16[32,64,128]{2,1,0:T(8,128)(2,1)S(1)}, u32[]{:S(2)}, u32[]{:S(2)}) async-start(bf16[32,64,128]{2,1,0:T(8,128)(2,1)} %bitcast.18), calls=%async_computation.3 | async-start | bytes 1048576 | tf_op jit(solution)/shard_map/all_to_all | solution.py:32
  279.3 14.2 %all-to-all-done.3 = bf16[32,64,128]{2,1,0:T(8,128)(2,1)S(1)} async-done(((bf16[32,64,128]{2,1,0:T(8,128)(2,1)}), bf16[32,64,128]{2,1,0:T(8,128)(2,1)S(1)}, u32[]{:S(2)}, u32[]{:S(2)}) %all-to-all-start.3) | async-done | bytes 524320 | tf_op jit(solution)/shard_map/all_to_all | solution.py:32
  (227 shorter events, 17.4 us)
Async XLA Ops:
  7.2 90.4 %copy-start = (bf16[1,128,2048]{2,1,0:T(8,128)(2,1)S(1)}, bf16[1,128,2048]{2,1,0:T(8,128)(2,1)}, u32[]{:S(2)}) copy-start(bf16[1,128,2048]{2,1,0:T(8,128)(2,1)} %param.19) | copy-start | bytes 1572868
  7.2 86.5 %all-gather.4.cloned.1.call-start = ((), (), s32[]{:S(2)}) async-start(), calls=%async_computation.5 | async-start | bytes 4456448 | tf_op jit(solution)/shard_map/all_gather | solution.py:17
  10.6 2.4 copy-start.16
  15.7 2.0 copy-start.8
  97.6 1.0 copy-start.4
  99.3 1.2 copy-start.5
  99.3 1.2 copy-start.17
  100.5 1.4 copy-start.1
  101.9 0.7 copy-start.10
  164.5 20.3 %all-to-all-start.2 = ((bf16[32,2,1024]{2,1,0:T(2,128)(2,1)}), bf16[32,2,1024]{2,1,0:T(2,128)(2,1)S(1)}, u32[]{:S(2)}, u32[]{:S(2)}) async-start(bf16[32,2,1024]{2,1,0:T(2,128)(2,1)} %reshape.296), calls=%async_computation.2 | async-start | bytes 262144 | tf_op jit(solution)/shard_map/all_to_all | solution.py:186
  174.4 71.9 %all-gather.6.cloned.1.call-start = ((), (), s32[]{:S(2)}) async-start(), calls=%async_computation.6 | async-start | bytes 8912896 | tf_op jit(solution)/shard_map/all_gather | solution.py:22
  187.7 3.5 %copy-start.12 = (f32[128,2]{1,0:T(8,128)S(1)}, f32[128,2]{1,0:T(8,128)}, u32[]{:S(2)}) copy-start(f32[128,2]{1,0:T(8,128)} %reshape.256) | copy-start | bytes 3076
  191.1 5.7 %copy-start.7 = (f32[128,128]{1,0:T(8,128)S(1)}, f32[128,128]{1,0:T(8,128)}, u32[]{:S(2)}) copy-start(f32[128,128]{1,0:T(8,128)} %param.16) | copy-start | bytes 196612
  191.1 7.0 %copy-start.15 = (f32[128,128]{1,0:T(8,128)S(1)}, f32[128,128]{1,0:T(8,128)}, u32[]{:S(2)}) copy-start(f32[128,128]{1,0:T(8,128)} %param.17) | copy-start | bytes 196612
  191.1 7.8 %copy-start.11 = (bf16[512,128]{1,0:T(8,128)(2,1)S(1)}, bf16[512,128]{1,0:T(8,128)(2,1)}, u32[]{:S(2)}) copy-start(bf16[512,128]{1,0:T(8,128)(2,1)} %copy-done.10) | copy-start | bytes 393220
  196.9 81.7 %collective-permute-start = (f32[1,128]{1,0:T(1,128)S(1)}, f32[1,128]{1,0:T(1,128)S(1)}, u32[]{:S(2)}, u32[]{:S(2)}) collective-permute-start(f32[1,128]{1,0:T(1,128)S(1)} %slice.423), channel_id=1, source_target_pairs={{0,16},{16,32},{32,48},{48,64},{64,80},{80,96},{96,112},{112,128},... | collective-permute-start | bytes 1544 | tf_op jit(solution)/shard_map/ppermute | solution.py:83
  198.9 2.6 copy-start.2
  198.9 2.5 copy-start.6
  246.4 5.4 %copy-start.3 = (bf16[128,2048]{1,0:T(8,128)(2,1)S(1)}, bf16[128,2048]{1,0:T(8,128)(2,1)}, u32[]{:S(2)}) copy-start(bf16[128,2048]{1,0:T(8,128)(2,1)} %param.12) | copy-start | bytes 1572868
  246.4 5.4 %copy-start.9 = (bf16[2048,128]{1,0:T(8,128)(2,1)S(1)}, bf16[2048,128]{1,0:T(8,128)(2,1)}, u32[]{:S(2)}) copy-start(bf16[2048,128]{1,0:T(8,128)(2,1)} %param.18) | copy-start | bytes 1572868
  246.4 5.4 %copy-start.13 = (bf16[128,128]{1,0:T(8,128)(2,1)S(1)}, bf16[128,128]{1,0:T(8,128)(2,1)}, u32[]{:S(2)}) copy-start(bf16[128,128]{1,0:T(8,128)(2,1)} %param.15) | copy-start | bytes 98308
  251.8 2.3 copy-start.14
  255.6 18.6 %all-to-all-start.4 = ((f32[32,2,128]{2,1,0:T(2,128)}), f32[32,2,128]{2,1,0:T(2,128)S(1)}, u32[]{:S(2)}, u32[]{:S(2)}) async-start(f32[32,2,128]{2,1,0:T(2,128)} %broadcast_in_dim.43), calls=%async_computation.4 | async-start | bytes 65536 | tf_op jit(solution)/shard_map/all_to_all | solution.py:38
  274.2 19.3 %all-to-all-start.3 = ((bf16[32,64,128]{2,1,0:T(8,128)(2,1)}), bf16[32,64,128]{2,1,0:T(8,128)(2,1)S(1)}, u32[]{:S(2)}, u32[]{:S(2)}) async-start(bf16[32,64,128]{2,1,0:T(8,128)(2,1)} %bitcast.18), calls=%async_computation.3 | async-start | bytes 1048576 | tf_op jit(solution)/shard_map/all_to_all | solution.py:32
Sparse Core Ops, SparseCore 0:
  51.6 42.0 all-gather.3
  196.9 49.3 all-gather.5
where the time goes:
time: 303 us; the launch traced here: 301 us
  waiting for transfers between devices  117 us (39%)
  blocking collectives  80.1 us (26%)
  local copies, waits for them, and re-layouts  34.1 us (11%)
  starting transfers between devices  25.3 us (8%)
  other arithmetic  20.1 us (7%)
  between operations  15.2 us (5%)
  matrix products  9.47 us (3%)
    all_to_all x1, blocking collectives, local(): lax.all_to_all(partial_value.reshape(slot_shape), 'tp', split_axis=2, con...  55.3 us
    all_gather x1, waiting for transfers between devices, gathered_total(): return lax.all_gather(shard, axis).astype(jnp.float32).sum(0)  43.6 us
    all_gather x1, waiting for transfers between devices, sent_together(): result = lax.all_gather(both, axis, axis=dim, tiled=True)  42.2 us
    all_to_all x1, blocking collectives, in_one_piece(): lax.all_to_all(both, axis, split_axis=split_dim, concat_axis=concat_dim,...  24.8 us
    all_to_all x1, waiting for transfers between devices, sum_at_owner(): lax.all_to_all(pieces, axis, split_axis=0, concat_axis=0, tiled=True)  14.2 us
    all_to_all x1, starting transfers between devices, local(): lax.all_to_all(summed.astype(jnp.bfloat16), 'sp', split_axis=1, concat_ax...  9.9 us
    all_to_all x1, starting transfers between devices, copy_for_each(): return lax.all_to_all(copies, axis, split_axis=0, concat_axis=0, tiled=True)  9.89 us
    all_to_all x1, waiting for transfers between devices, local(): lax.all_to_all(summed.astype(jnp.bfloat16), 'sp', split_axis=1, concat_ax...  9.31 us
  transfers between devices with their start and end apart: 6, of which 5 were waited for; matrix products, arithmetic and copies ran while one was open for 5% of the time, Pallas kernels for 0%

commit v1 on v0

v1 whole, which is shorter than its diff:
```python
import functools
import jax
import jax.numpy as jnp
from jax import lax
from jax.experimental import pallas as pl
from jax.experimental.pallas import tpu as pltpu
from jax.sharding import PartitionSpec as P

F32 = jnp.float32
BF16 = jnp.bfloat16
LANES = 128
MESH = pl.DeviceIdType.MESH


def dot(a, b, contract=((1,), (0,))):
    return lax.dot_general(a, b, (contract, ((), ())), preferred_element_type=F32)


def shift_up(a, k, fill):
    pad = jnp.full((k, a.shape[1]), fill, a.dtype)
    return jnp.concatenate([a[k:], pad], axis=0)


def kernel(
    sizes,
    ids, wts, mix, outg, gbr, st, dec, wp, wg, wu, wd,
    o_gate, o_up, o_down, o_proj, o_branch, o_drive, o_decay,
    onehot_s, disp, xc, acc_gu, acc_h, act_s, pbuf, precv, sbuf, rbuf, fin, ret, mid_all,
    gp_send, gp_recv, car_send, car_recv, prev_b,
    s1, r1, rs, ds, rr, ps, pr, cs, cr, fs, fr, ms, mf, mr, gs, gr, ks, kr, vs, vr,
):
    SP, TP, CAP = sizes
    Y = TP // 2
    H = Y // 2
    SH = SP // 2
    n = mix.shape[0]
    d_model = mix.shape[1]
    slots = SP * CAP
    me = lax.axis_index("sp")
    t = lax.axis_index("tp")
    y = t // 2
    core = t % 2
    partner = t + 1 - 2 * core
    right = (t + 2) % TP
    left = (t + TP - 2) % TP

    def chip(off):
        return (y + off + Y) % Y

    def remote(src, dst, send, recv, **device):
        return pltpu.make_async_remote_copy(
            src_ref=src, dst_ref=dst, send_sem=send, recv_sem=recv,
            device_id=device, device_id_type=MESH,
        )

    def each_peer(body):
        def step(i, carry):
            body((me + 1 + i) % SP)
            return carry

        lax.fori_loop(0, SP - 1, step, 0)

    barrier = pltpu.get_barrier_semaphore()
    each_peer(
        lambda p: pl.semaphore_signal(barrier, inc=1, device_id={"sp": p}, device_id_type=MESH)
    )
    for off in range(1, Y):
        pl.semaphore_signal(
            barrier, inc=1, device_id={"tp": (t + 2 * off) % TP}, device_id_type=MESH
        )
    pl.semaphore_signal(barrier, inc=1, device_id={"tp": partner}, device_id_type=MESH)

    own_cols = pl.ds(pl.multiple_of(t * LANES, LANES), LANES)
    expert_io = lax.broadcasted_iota(jnp.int32, (SP, n), 0)
    hots = [(expert_io == ids[k : k + 1, :]).astype(F32) for k in range(2)]
    earlier = (
        lax.broadcasted_iota(jnp.int32, (n, n), 0) < lax.broadcasted_iota(jnp.int32, (n, n), 1)
    ).astype(F32).astype(BF16)
    before = dot((hots[0] + hots[1]).astype(BF16), earlier)
    slot_io = lax.broadcasted_iota(jnp.int32, (slots, n), 0).astype(F32)
    picks = []
    for k in range(2):
        pos = jnp.sum(hots[k] * before, axis=0, keepdims=True)
        picks.append(slot_io == ids[k : k + 1, :].astype(F32) * float(CAP) + pos)
    onehot = (picks[0] | picks[1]).astype(F32).astype(BF16)
    onehot_s[...] = onehot
    weight = jnp.sum(
        jnp.where(picks[0], wts[0:1, :], 0.0) + jnp.where(picks[1], wts[1:2, :], 0.0),
        axis=1, keepdims=True,
    )
    x_slots = dot(onehot, mix[:, own_cols]).astype(BF16)
    c_slots = (weight * dot(onehot, outg[:, own_cols])).astype(BF16)
    disp[:, 0:CAP, :] = x_slots.reshape(SP, CAP, LANES)
    disp[:, CAP : 2 * CAP, :] = c_slots.reshape(SP, CAP, LANES)
    xc[t, me] = disp[me]

    pl.semaphore_wait(barrier, SP - 1 + Y)

    def dispatch(p):
        return remote(disp.at[p], xc.at[t, me], s1.at[p], r1.at[me], sp=p)

    each_peer(lambda p: dispatch(p).start())
    last_state = remote(
        st.at[pl.ds(n - 8, 8)], prev_b, vs.at[0], vr.at[0], sp=(me + 1) % SP
    )
    last_state.start()

    def arrived_1(half):
        def step(i, carry):
            b = half * SH + i

            @pl.when(b != me)
            def _():
                remote(disp.at[b], xc.at[t, b], s1.at[b], r1.at[b], sp=b).wait_recv()

            return carry

        lax.fori_loop(0, SH, step, 0)

    def half_of(src, h):
        return xc.at[src, pl.ds(h * SH, SH)]

    def ring(src, h, way, step):
        dev = right if way == 0 else left
        return remote(half_of(src, h), half_of(src, h), rs.at[way, h, step], rr.at[src, h], tp=dev)

    def across(src, h):
        return remote(
            half_of(src, h), half_of(src, h), ds.at[src // 2, h], rr.at[src, h], tp=partner
        )

    acc_gu[...] = jnp.zeros_like(acc_gu)
    acc_h[...] = jnp.zeros_like(acc_h)

    def pair_of(yy, part):
        lo, hi = (0, CAP) if part == 0 else (CAP, 2 * CAP)
        return jnp.concatenate(
            [xc[2 * yy + k, :, lo:hi, :].reshape(slots, LANES) for k in range(2)], axis=1
        )

    def cols_of(yy):
        return pl.ds(pl.multiple_of(yy * 2 * LANES, 2 * LANES), 2 * LANES)

    def forward(yy):
        other = 2 * yy + 1 - core
        for h in range(2):
            across(other, h).wait_recv()
        cols = cols_of(yy)
        w_in = jnp.concatenate([wg[:, cols], wu[:, cols]], axis=0)
        acc_gu[...] += dot(pair_of(yy, 0), w_in, ((1,), (1,)))
        acc_h[...] += dot(pair_of(yy, 1), wd[:, cols], ((1,), (1,)))

    for h in range(2):
        arrived_1(h)
        for way in range(2):
            ring(t, h, way, 0).start()
        across(t, h).start()

    for s in range(1, H + 1):
        for way, h in ((0, 0), (1, 1), (1, 0), (0, 1)):
            most = H if way == h else H - 1
            if s > most:
                continue
            src = 2 * chip(-s if way == 0 else s) + core
            ring(src, h, way, s - 1).wait_recv()
            if s < most:
                ring(src, h, way, s).start()
            across(src, h).start()
        forward(chip(s - 1))
        if s > 1:
            forward(chip(1 - s))
    forward(chip(H))

    gate = acc_gu[:, 0:LANES]
    up = acc_gu[:, LANES : 2 * LANES]
    hg = acc_h[...]
    sig = jax.nn.sigmoid(gate)
    silu = gate * sig
    hidden = (silu * up).astype(BF16)
    up_grad = (hg * silu).astype(BF16)
    gate_grad = (hg * up * sig * (1.0 + gate * (1.0 - sig))).astype(BF16)
    grads = jnp.concatenate([gate_grad, up_grad], axis=1)

    def partial(off):
        yy = chip(off)
        cols = cols_of(yy)
        value = dot(grads, jnp.concatenate([wg[:, cols], wu[:, cols]], axis=0)).astype(BF16)
        pbuf[yy, 0] = value[:, 0:LANES]
        pbuf[yy, 1] = value[:, LANES : 2 * LANES]
        swap(yy).start()

    def swap(yy):
        return remote(pbuf.at[yy, 1 - core], precv.at[yy], ps.at[yy], pr.at[yy], tp=partner)

    rows = slots // 2

    def own_sum(off, h):
        yy = chip(off)
        part = pl.ds(h * rows, rows)
        return pbuf[yy, core, part, :].astype(F32) + precv[yy, part, :].astype(F32)

    def chain(way, h, step):
        dev = right if way == 0 else left
        return remote(
            sbuf.at[way, h, step], rbuf.at[way, h, step],
            cs.at[way, h, step], cr.at[way, h, step], tp=dev,
        )

    flows = ((0, 0), (1, 1), (0, 1), (1, 0))

    def length(way, h):
        return H if way == h else H - 1

    def sign(way):
        return 1 if way == 0 else -1

    partial(H)
    partial(H - 1)
    partial(1 - H)
    swap(chip(H)).wait_recv()
    for way, h in flows[:2]:
        sbuf[way, h, 0] = own_sum(H, h).astype(BF16)
        chain(way, h, 0).start()
    for way, h in flows[2:]:
        off = sign(way) * (H - 1)
        swap(chip(off)).wait_recv()
        sbuf[way, h, 0] = own_sum(off, h).astype(BF16)
        chain(way, h, 0).start()
    for m in range(H - 2, 0, -1):
        partial(m)
        partial(-m)
    partial(0)
    for m in range(H - 2, 0, -1):
        swap(chip(m)).wait_recv()
        swap(chip(-m)).wait_recv()
    swap(chip(0)).wait_recv()

    grads_t = grads.T
    hidden_t = hidden.T

    def weight_grads(yy):
        cols = cols_of(yy)
        both = dot(grads_t, pair_of(yy, 0)).astype(BF16)
        o_gate[:, cols] = both[0:LANES]
        o_up[:, cols] = both[LANES : 2 * LANES]
        o_down[:, cols] = dot(hidden_t, pair_of(yy, 1)).astype(BF16)

    todo = list(range(Y))
    per_step = -(-Y // H)
    for s in range(1, H):
        for _ in range(per_step):
            if todo:
                weight_grads(todo.pop(0))
        for way, h in flows:
            most = length(way, h)
            if s >= most:
                continue
            off = sign(way) * (most - s)
            chain(way, h, s - 1).wait_recv()
            sbuf[way, h, s] = (rbuf[way, h, s - 1].astype(F32) + own_sum(off, h)).astype(BF16)
            chain(way, h, s).start()
    while todo:
        weight_grads(todo.pop(0))

    def give(p):
        return remote(fin.at[p], ret.at[me], fs.at[p], fr.at[me], sp=p)

    for h in range(2):
        total = own_sum(0, h)
        for way in range(2):
            step = length(way, h) - 1
            chain(way, h, step).wait_recv()
            total = total + rbuf[way, h, step].astype(F32)
        fin[pl.ds(h * SH, SH)] = total.astype(BF16).reshape(SH, CAP, LANES)

        def send_back(i, carry):
            b = h * SH + i

            @pl.when(b != me)
            def _():
                give(b).start()

            return carry

        lax.fori_loop(0, SH, send_back, 0)
    ret[me] = fin[me]

    onehot_t = onehot_s[...].T
    out_cols = outg[:, own_cols].astype(F32)
    gated = (gbr[...].astype(F32) * st[...]).astype(BF16)
    prod = shift_up(dec[...], 1, 1.0)
    shifts = [1 << k for k in range((n - 1).bit_length())]
    prods = []
    for k in shifts:
        prods.append(prod)
        prod = prod * shift_up(prod, k, 1.0)

    each_peer(lambda p: remote(fin.at[p], ret.at[p], fs.at[p], fr.at[p], sp=p).wait_recv())
    routed = dot(onehot_t, ret[...].reshape(slots, LANES))
    mid_all[t] = (out_cols + routed).astype(BF16)

    def share(off):
        return remote(
            mid_all.at[t], mid_all.at[t], ms.at[off], mr.at[t], tp=(t + 2 * off) % TP
        )

    def pass_mid(src):
        return remote(mid_all.at[src], mid_all.at[src], mf.at[src // 2], mr.at[src], tp=partner)

    order = [off for m in range(1, H) for off in (m, -m)] + [H]
    pass_mid(t).start()
    for off in order:
        share(off % Y).start()

    block = d_model // SP
    per_chip = 2 * LANES // block

    def give_proj(p):
        return remote(gp_send.at[p], gp_recv.at[me], gs.at[p], gr.at[me], sp=p)

    def project(yy):
        pass_mid(2 * yy + 1 - core).wait_recv()
        mid = jnp.concatenate([mid_all[2 * yy], mid_all[2 * yy + 1]], axis=1)
        part = dot(mid.T, gated).astype(BF16)
        for j in range(per_chip):
            owner = yy * per_chip + j
            gp_send[owner] = part[j * block : (j + 1) * block]

            @pl.when(owner != me)
            def _():
                give_proj(owner).start()

        return dot(mid, wp[cols_of(yy), :])

    act = None
    queue = [0]
    for off in order:
        src = 2 * chip(off) + core
        remote(mid_all.at[src], mid_all.at[src], mf.at[0], mr.at[src], tp=partner).wait_recv()
        pass_mid(src).start()
        ready = queue.pop(0)
        term = project(chip(ready))
        act = term if act is None else act + term
        queue.append(off)
    for off in queue:
        act = act + project(chip(off))
    gp_recv[me] = gp_send[me]

    states = st[...]
    o_branch[...] = (act * states).astype(BF16)
    grad = act * gbr[...].astype(F32)
    for k, a in zip(shifts, prods):
        grad = grad + a * shift_up(grad, k, 0.0)

    head = dec[0:1, :]
    car_send[0:1, :] = head * prod[0:1, :]
    car_send[1:2, :] = head * grad[0:1, :]

    def carry_to(p):
        return remote(car_send, car_recv.at[me], ks.at[p], kr.at[me], sp=p)

    each_peer(lambda p: carry_to(p).start())
    car_recv[me] = car_send[...]
    each_peer(lambda p: remote(car_send, car_recv.at[p], ks.at[p], kr.at[p], sp=p).wait_recv())

    def enter(i, value):
        b = SP - 1 - i
        pair = car_recv[b]
        later = jnp.where(b > me, 1.0, 0.0)
        return later * (pair[1:2, :] + pair[0:1, :] * value) + (1.0 - later) * value

    entering = lax.fori_loop(0, SP - 1, enter, jnp.zeros((1, LANES), F32))
    drive = grad + prod * entering
    o_drive[...] = drive
    last_state.wait_recv()
    first = jnp.where(me > 0, 1.0, 0.0) * prev_b[7:8, :]
    o_decay[...] = drive * jnp.concatenate([first, states[: n - 1]], axis=0)

    each_peer(lambda p: remote(gp_send.at[p], gp_recv.at[p], gs.at[p], gr.at[p], sp=p).wait_recv())

    def add(b, total):
        return total + gp_recv[b].astype(F32)

    o_proj[...] = lax.fori_loop(0, SP, add, jnp.zeros((block, LANES), F32))

    def drain(p):
        dispatch(p).wait_send()
        give(p).wait_send()
        give_proj(p).wait_send()
        carry_to(p).wait_send()

    each_peer(drain)
    last_state.wait_send()
    for way in range(2):
        for h in range(2):
            most = length(way, h)
            for s in range(most):
                ring(t, h, way, s).wait_send()
                chain(way, h, s).wait_send()
    for yy in range(Y):
        for h in range(2):
            across(2 * yy + core, h).wait_send()
        swap(yy).wait_send()
        pass_mid(2 * yy + core).wait_send()
    for off in range(1, Y):
        share(off).wait_send()


def local(
    mixer_out, out_grad, route_ids, route_weights, gate_branch, states, decay, w_proj,
    w_gate, w_up, w_down,
):
    n, d_model = mixer_out.shape
    SP = lax.axis_size("sp")
    TP = lax.axis_size("tp")
    Y, H = TP // 2, TP // 4
    CAP = min(n, 2 * route_ids.shape[1] * n // SP)
    slots = SP * CAP
    block = d_model // SP
    dma = pltpu.SemaphoreType.DMA
    big = jax.ShapeDtypeStruct((LANES, d_model), BF16)
    vmem = pl.BlockSpec(memory_space=pltpu.VMEM)
    outs = pl.pallas_call(
        functools.partial(kernel, (SP, TP, CAP)),
        out_shape=(
            big, big, big,
            jax.ShapeDtypeStruct((block, LANES), F32),
            jax.ShapeDtypeStruct((n, LANES), BF16),
            jax.ShapeDtypeStruct((n, LANES), F32),
            jax.ShapeDtypeStruct((n, LANES), F32),
        ),
        in_specs=[vmem] * 11,
        out_specs=(vmem,) * 7,
        scratch_shapes=[
            pltpu.VMEM((slots, n), BF16),
            pltpu.VMEM((SP, 2 * CAP, LANES), BF16),
            pltpu.VMEM((TP, SP, 2 * CAP, LANES), BF16),
            pltpu.VMEM((slots, 2 * LANES), F32),
            pltpu.VMEM((slots, LANES), F32),
            pltpu.VMEM((n, LANES), F32),
            pltpu.VMEM((Y, 2, slots, LANES), BF16),
            pltpu.VMEM((Y, slots, LANES), BF16),
            pltpu.VMEM((2, 2, H, slots // 2, LANES), BF16),
            pltpu.VMEM((2, 2, H, slots // 2, LANES), BF16),
            pltpu.VMEM((SP, CAP, LANES), BF16),
            pltpu.VMEM((SP, CAP, LANES), BF16),
            pltpu.VMEM((TP, n, LANES), BF16),
            pltpu.VMEM((SP, block, LANES), BF16),
            pltpu.VMEM((SP, block, LANES), BF16),
            pltpu.VMEM((2, LANES), F32),
            pltpu.VMEM((SP, 2, LANES), F32),
            pltpu.VMEM((8, LANES), F32),
            dma((SP,)), dma((SP,)),
            dma((2, 2, H)), dma((Y, 2)), dma((TP, 2)),
            dma((Y,)), dma((Y,)),
            dma((2, 2, H)), dma((2, 2, H)),
            dma((SP,)), dma((SP,)),
            dma((Y,)), dma((Y,)), dma((TP,)),
            dma((SP,)), dma((SP,)),
            dma((SP,)), dma((SP,)),
            dma((1,)), dma((1,)),
        ],
        compiler_params=pltpu.CompilerParams(
            collective_id=0, has_side_effects=True, vmem_limit_bytes=48 * 1024 * 1024
        ),
    )(
        route_ids.T, route_weights.T, mixer_out, out_grad, gate_branch, states, decay, w_proj,
        w_gate[0], w_up[0], w_down[0],
    )
    return (outs[0][None], outs[1][None], outs[2][None], *outs[3:])


def solution(mesh):
    placed = (
        P("sp", None),
        P("sp", None),
        P("sp", None),
        P("sp", None),
        P("sp", "tp"),
        P("sp", "tp"),
        P("sp", "tp"),
        P(None, "tp"),
        P("sp", "tp", None),
        P("sp", "tp", None),
        P("sp", "tp", None),
    )
    return jax.shard_map(
        local,
        mesh=mesh,
        in_specs=placed,
        out_specs=(
            P("sp", "tp", None),
            P("sp", "tp", None),
            P("sp", "tp", None),
            P("sp", "tp"),
            P("sp", "tp"),
            P("sp", "tp"),
            P("sp", "tp"),
        ),
        check_vma=False,
    )
```

time: 303 us -> 114 us (0.38)
  the two profiles are of different devices: /device:TPU:1 before, /device:TPU:25 now
where the time goes in v1:
time: 114 us
  Pallas kernels  99 us (87%)
  local copies, waits for them, and re-layouts  14.2 us (12%)
    pallas_call x1, Pallas kernels, local(): pl.pallas_call(functools.partial(kernel, (SP, TP, CAP)), out_shape=(big,...  99 us
    unnamed x29, local copies, waits for them, and re-layouts  14.2 us

profile of v1, /device:TPU:25, one launch (start us, length us, event | category | flops | bytes accessed | tf_op | source)
XLA Modules:
  0.0 113.9 jit_solution(7631802204206412854)
XLA Ops:
  0.6 0.0 copy-start.10
  0.6 0.0 copy-start.9
  0.7 0.7 copy-done.10
  1.3 0.0 copy-done.9
  1.3 0.0 copy-start
  1.3 1.0 copy-done
  2.4 0.0 copy-start.1
  2.4 1.0 copy-done.1
  3.4 0.0 copy-start.2
  3.4 1.0 copy-done.2
  4.5 0.0 copy-start.3
  4.5 1.0 copy-done.3
  5.5 0.0 copy-start.4
  5.5 1.0 copy-done.4
  6.5 0.0 copy-start.5
  6.5 1.0 copy-done.5
  7.6 0.0 copy-start.6
  7.6 0.8 copy-done.6
  8.4 0.0 copy-start.7
  8.4 0.8 copy-done.7
  9.3 0.0 copy-start.8
  9.3 0.8 copy-done.8
  10.0 99.0 %shard_map.162 = (bf16[128,2048]{1,0:T(8,128)(2,1)S(1)}, bf16[128,2048]{1,0:T(8,128)(2,1)S(1)}, bf16[128,2048]{1,0:T(8,128)(2,1)S(1)}, f32[64,128]{1,0:T(8,128)S...) custom-call(s32[2,128]{1,0:T(2,128)S(1)} %bitcast.14, f32[2,128]{1,0:T(2,128)S(1)} %bitcast.15, ...), custom_call_target="tpu_custom_call" | custom-call | tf_op jit(solution)/shard_map/pallas_call | solution.py:423
  109.0 0.8 copy.25
  109.8 0.8 copy.26
  110.6 0.8 copy.27
  111.4 0.6 copy.28
  112.0 0.6 copy.29
  112.6 0.6 copy.30
  113.2 0.6 copy.31
Async XLA Ops:
  0.6 0.7 copy-start.10
  0.6 0.7 copy-start.9
  1.3 1.0 copy-start
  2.4 1.0 copy-start.1
  3.4 1.0 copy-start.2
  4.5 1.0 copy-start.3
  5.5 1.0 copy-start.4
  6.5 1.0 copy-start.5
  7.6 0.8 copy-start.6
  8.4 0.8 copy-start.7
  9.3 0.8 copy-start.8

commit v2 on v1

--- a/solution.py
+++ b/solution.py
@@ -23,18 +23,19 @@
 
 def kernel(
     sizes,
+    ids_h, wts_h, mix_h, outg_h, gbr_h, st_h, dec_h, wp_h, wg_h, wu_h, wd_h,
+    o_gate, o_up, o_down, o_proj, o_branch, o_drive, o_decay,
     ids, wts, mix, outg, gbr, st, dec, wp, wg, wu, wd,
-    o_gate, o_up, o_down, o_proj, o_branch, o_drive, o_decay,
-    onehot_s, disp, xc, acc_gu, acc_h, act_s, pbuf, precv, sbuf, rbuf, fin, ret, mid_all,
-    gp_send, gp_recv, car_send, car_recv, prev_b,
-    s1, r1, rs, ds, rr, ps, pr, cs, cr, fs, fr, ms, mf, mr, gs, gr, ks, kr, vs, vr,
+    onehot_s, disp, xc, acc_gu, acc_h, pbuf, precv, sbuf, rbuf, fin, ret, mid_all,
+    gx_send, gx_recv, gz_send, gz_recv, car_send, car_recv, prev_b,
+    ins, s1, r1, rs, ds, rr, ps, pr, cs, cr, fs, fr, ms, mf, mr, xs, xr, zs, zr, ks, kr, vs, vr,
 ):
-    SP, TP, CAP = sizes
+    SP, X, TP, CAP = sizes
     Y = TP // 2
     H = Y // 2
     SH = SP // 2
-    n = mix.shape[0]
-    d_model = mix.shape[1]
+    n = mix_h.shape[0]
+    d_model = mix_h.shape[1]
     slots = SP * CAP
     me = lax.axis_index("sp")
     t = lax.axis_index("tp")
@@ -71,6 +72,21 @@
     pl.semaphore_signal(barrier, inc=1, device_id={"tp": partner}, device_id_type=MESH)
 
     own_cols = pl.ds(pl.multiple_of(t * LANES, LANES), LANES)
+    fetch = [
+        pltpu.make_async_copy(src, dst, ins.at[k])
+        for k, (src, dst) in enumerate(
+            (
+                (ids_h, ids), (wts_h, wts), (mix_h.at[:, own_cols], mix),
+                (outg_h.at[:, own_cols], outg), (st_h, st), (wg_h, wg), (wu_h, wu), (wd_h, wd),
+                (gbr_h, gbr), (dec_h, dec), (wp_h, wp),
+            )
+        )
+    ]
+    for copy in fetch:
+        copy.start()
+    for copy in fetch[:4]:
+        copy.wait()
+
     expert_io = lax.broadcasted_iota(jnp.int32, (SP, n), 0)
     hots = [(expert_io == ids[k : k + 1, :]).astype(F32) for k in range(2)]
     earlier = (
@@ -88,8 +104,8 @@
         jnp.where(picks[0], wts[0:1, :], 0.0) + jnp.where(picks[1], wts[1:2, :], 0.0),
         axis=1, keepdims=True,
     )
-    x_slots = dot(onehot, mix[:, own_cols]).astype(BF16)
-    c_slots = (weight * dot(onehot, outg[:, own_cols])).astype(BF16)
+    x_slots = dot(onehot, mix[...]).astype(BF16)
+    c_slots = (weight * dot(onehot, outg[...])).astype(BF16)
     disp[:, 0:CAP, :] = x_slots.reshape(SP, CAP, LANES)
     disp[:, CAP : 2 * CAP, :] = c_slots.reshape(SP, CAP, LANES)
     xc[t, me] = disp[me]
@@ -100,6 +116,8 @@
         return remote(disp.at[p], xc.at[t, me], s1.at[p], r1.at[me], sp=p)
 
     each_peer(lambda p: dispatch(p).start())
+    for copy in fetch[4:]:
+        copy.wait()
     last_state = remote(
         st.at[pl.ds(n - 8, 8)], prev_b, vs.at[0], vr.at[0], sp=(me + 1) % SP
     )
@@ -286,7 +304,7 @@
     ret[me] = fin[me]
 
     onehot_t = onehot_s[...].T
-    out_cols = outg[:, own_cols].astype(F32)
+    out_cols = outg[...].astype(F32)
     gated = (gbr[...].astype(F32) * st[...]).astype(BF16)
     prod = shift_up(dec[...], 1, 1.0)
     shifts = [1 << k for k in range((n - 1).bit_length())]
@@ -309,31 +327,51 @@
 
     order = [off for m in range(1, H) for off in (m, -m)] + [H]
     pass_mid(t).start()
-    for off in order:
+    for off in order[::-1]:
         share(off % Y).start()
 
     block = d_model // SP
-    per_chip = 2 * LANES // block
-
-    def give_proj(p):
-        return remote(gp_send.at[p], gp_recv.at[me], gs.at[p], gr.at[me], sp=p)
+    z = me // X
+    x = me % X
+
+    def over_x(yy, j):
+        return remote(
+            gx_send.at[yy, j], gx_recv.at[yy, x], xs.at[yy, j], xr.at[yy, x], sp=z * X + j
+        )
+
+    def over_z(yy):
+        return remote(gz_send.at[yy], gz_recv.at[z], zs.at[yy], zr.at[z], sp=yy * X + x)
+
+    def x_peers(body):
+        for j in range(1, X):
+            body((x + j) % X)
 
     def project(yy):
         pass_mid(2 * yy + 1 - core).wait_recv()
         mid = jnp.concatenate([mid_all[2 * yy], mid_all[2 * yy + 1]], axis=1)
         part = dot(mid.T, gated).astype(BF16)
-        for j in range(per_chip):
-            owner = yy * per_chip + j
-            gp_send[owner] = part[j * block : (j + 1) * block]
-
-            @pl.when(owner != me)
-            def _():
-                give_proj(owner).start()
-
+        gx_send[yy] = part.reshape(X, block, LANES)
+        x_peers(lambda j: over_x(yy, j).start())
         return dot(mid, wp[cols_of(yy), :])
+
+    def forward_proj(yy):
+        total = gx_send[yy, x].astype(F32)
+        for j in range(1, X):
+            src = (x + j) % X
+            remote(
+                gx_send.at[yy, src], gx_recv.at[yy, src], xs.at[yy, src], xr.at[yy, src],
+                sp=z * X + src,
+            ).wait_recv()
+            total = total + gx_recv[yy, src].astype(F32)
+        gz_send[yy] = total.astype(BF16)
+
+        @pl.when(yy != z)
+        def _():
+            over_z(yy).start()
 
     act = None
     queue = [0]
+    behind = []
     for off in order:
         src = 2 * chip(off) + core
         remote(mid_all.at[src], mid_all.at[src], mf.at[0], mr.at[src], tp=partner).wait_recv()
@@ -342,9 +380,12 @@
         term = project(chip(ready))
         act = term if act is None else act + term
         queue.append(off)
+        behind.append(ready)
+        if len(behind) > 2:
+            forward_proj(chip(behind.pop(0)))
     for off in queue:
         act = act + project(chip(off))
-    gp_recv[me] = gp_send[me]
+        behind.append(off)
 
     states = st[...]
     o_branch[...] = (act * states).astype(BF16)
@@ -360,6 +401,8 @@
         return remote(car_send, car_recv.at[me], ks.at[p], kr.at[me], sp=p)
 
     each_peer(lambda p: carry_to(p).start())
+    for off in behind:
+        forward_proj(chip(off))
     car_recv[me] = car_send[...]
     each_peer(lambda p: remote(car_send, car_recv.at[p], ks.at[p], kr.at[p], sp=p).wait_recv())
 
@@ -376,21 +419,33 @@
     first = jnp.where(me > 0, 1.0, 0.0) * prev_b[7:8, :]
     o_decay[...] = drive * jnp.concatenate([first, states[: n - 1]], axis=0)
 
-    each_peer(lambda p: remote(gp_send.at[p], gp_recv.at[p], gs.at[p], gr.at[p], sp=p).wait_recv())
-
-    def add(b, total):
-        return total + gp_recv[b].astype(F32)
-
-    o_proj[...] = lax.fori_loop(0, SP, add, jnp.zeros((block, LANES), F32))
+    def z_peers(body):
+        def step(i, carry):
+            body((z + 1 + i) % Y)
+            return carry
+
+        lax.fori_loop(0, Y - 1, step, 0)
+
+    z_peers(
+        lambda p: remote(
+            gz_send.at[p], gz_recv.at[p], zs.at[p], zr.at[p], sp=p * X + x
+        ).wait_recv()
+    )
+    total = gz_send[z].astype(F32)
+    for i in range(1, Y):
+        total = total + gz_recv[(z + i) % Y].astype(F32)
+    o_proj[...] = total
 
     def drain(p):
         dispatch(p).wait_send()
         give(p).wait_send()
-        give_proj(p).wait_send()
         carry_to(p).wait_send()
 
     each_peer(drain)
     last_state.wait_send()
+    z_peers(lambda p: over_z(p).wait_send())
+    for yy in range(Y):
+        x_peers(lambda j: over_x(yy, j).wait_send())
     for way in range(2):
         for h in range(2):
             most = length(way, h)
@@ -406,6 +461,17 @@
         share(off).wait_send()
 
 
+def store(*refs):
+    count = len(refs) // 2
+    copies = [
+        pltpu.make_async_copy(refs[k], refs[count + k], refs[-1].at[k]) for k in range(count)
+    ]
+    for copy in copies:
+        copy.start()
+    for copy in copies:
+        copy.wait()
+
+
 def local(
     mixer_out, out_grad, route_ids, route_weights, gate_branch, states, decay, w_proj,
     w_gate, w_up, w_down,
@@ -416,12 +482,13 @@
     Y, H = TP // 2, TP // 4
     CAP = min(n, 2 * route_ids.shape[1] * n // SP)
     slots = SP * CAP
+    X = SP // Y
     block = d_model // SP
     dma = pltpu.SemaphoreType.DMA
     big = jax.ShapeDtypeStruct((LANES, d_model), BF16)
     vmem = pl.BlockSpec(memory_space=pltpu.VMEM)
     outs = pl.pallas_call(
-        functools.partial(kernel, (SP, TP, CAP)),
+        functools.partial(kernel, (SP, SP // Y, TP, CAP)),
         out_shape=(
             big, big, big,
             jax.ShapeDtypeStruct((block, LANES), F32),
@@ -429,15 +496,25 @@
             jax.ShapeDtypeStruct((n, LANES), F32),
             jax.ShapeDtypeStruct((n, LANES), F32),
         ),
-        in_specs=[vmem] * 11,
+        in_specs=[pl.BlockSpec(memory_space=pltpu.HBM)] * 11,
         out_specs=(vmem,) * 7,
         scratch_shapes=[
+            pltpu.VMEM((2, n), jnp.int32),
+            pltpu.VMEM((2, n), F32),
+            pltpu.VMEM((n, LANES), BF16),
+            pltpu.VMEM((n, LANES), BF16),
+            pltpu.VMEM((n, LANES), BF16),
+            pltpu.VMEM((n, LANES), F32),
+            pltpu.VMEM((n, LANES), F32),
+            pltpu.VMEM((d_model, LANES), BF16),
+            pltpu.VMEM((LANES, d_model), BF16),
+            pltpu.VMEM((LANES, d_model), BF16),
+            pltpu.VMEM((LANES, d_model), BF16),
             pltpu.VMEM((slots, n), BF16),
             pltpu.VMEM((SP, 2 * CAP, LANES), BF16),
             pltpu.VMEM((TP, SP, 2 * CAP, LANES), BF16),
             pltpu.VMEM((slots, 2 * LANES), F32),
             pltpu.VMEM((slots, LANES), F32),
-            pltpu.VMEM((n, LANES), F32),
             pltpu.VMEM((Y, 2, slots, LANES), BF16),
             pltpu.VMEM((Y, slots, LANES), BF16),
             pltpu.VMEM((2, 2, H, slots // 2, LANES), BF16),
@@ -445,28 +522,37 @@
             pltpu.VMEM((SP, CAP, LANES), BF16),
             pltpu.VMEM((SP, CAP, LANES), BF16),
             pltpu.VMEM((TP, n, LANES), BF16),
-            pltpu.VMEM((SP, block, LANES), BF16),
-            pltpu.VMEM((SP, block, LANES), BF16),
+            pltpu.VMEM((Y, X, block, LANES), BF16),
+            pltpu.VMEM((Y, X, block, LANES), BF16),
+            pltpu.VMEM((Y, block, LANES), BF16),
+            pltpu.VMEM((Y, block, LANES), BF16),
             pltpu.VMEM((2, LANES), F32),
             pltpu.VMEM((SP, 2, LANES), F32),
             pltpu.VMEM((8, LANES), F32),
-            dma((SP,)), dma((SP,)),
+            dma((11,)), dma((SP,)), dma((SP,)),
             dma((2, 2, H)), dma((Y, 2)), dma((TP, 2)),
             dma((Y,)), dma((Y,)),
             dma((2, 2, H)), dma((2, 2, H)),
             dma((SP,)), dma((SP,)),
             dma((Y,)), dma((Y,)), dma((TP,)),
-            dma((SP,)), dma((SP,)),
+            dma((Y, X)), dma((Y, X)), dma((Y,)), dma((Y,)),
             dma((SP,)), dma((SP,)),
             dma((1,)), dma((1,)),
         ],
         compiler_params=pltpu.CompilerParams(
             collective_id=0, has_side_effects=True, vmem_limit_bytes=48 * 1024 * 1024
         ),
-    )(
+    )(*(pltpu.with_memory_space_constraint(a, pltpu.HBM) for a in (
         route_ids.T, route_weights.T, mixer_out, out_grad, gate_branch, states, decay, w_proj,
         w_gate[0], w_up[0], w_down[0],
-    )
+    )))
+    outs = pl.pallas_call(
+        store,
+        out_shape=tuple(jax.ShapeDtypeStruct(o.shape, o.dtype) for o in outs),
+        in_specs=[vmem] * len(outs),
+        out_specs=(pl.BlockSpec(memory_space=pltpu.HBM),) * len(outs),
+        scratch_shapes=[dma((len(outs),))], compiler_params=pltpu.CompilerParams(vmem_limit_bytes=4194304),
+    )(*outs)
     return (outs[0][None], outs[1][None], outs[2][None], *outs[3:])
 
 

time: 114 us -> 98.8 us (0.87)
  the two profiles are of different devices: /device:TPU:25 before, /device:TPU:1 now
where the time goes in v2:
time: 98.8 us; the launch traced here: 98.3 us
  Pallas kernels  97.6 us (99%)
    pallas_call x1, Pallas kernels, local(): pl.pallas_call(functools.partial(kernel, (SP, SP // Y, TP, CAP)), out_sha...  96.4 us

profile of v2, /device:TPU:1, one launch (start us, length us, event | category | flops | bytes accessed | tf_op | source)
XLA Modules:
  0.0 98.3 jit_solution(15965865602673632859)
XLA Ops:
  0.6 96.4 %shard_map.162 = (bf16[128,2048]{1,0:T(8,128)(2,1)S(1)}, bf16[128,2048]{1,0:T(8,128)(2,1)S(1)}, bf16[128,2048]{1,0:T(8,128)(2,1)S(1)}, f32[64,128]{1,0:T(8,128)S...) custom-call(s32[2,128]{1,0:T(2,128)} %bitcast.11, f32[2,128]{1,0:T(2,128)} %bitcast.12, ...), custom_call_target="tpu_custom_call" | custom-call | tf_op jit(solution)/shard_map/pallas_call | solution.py:490
  97.0 1.3 %shard_map.163 = (bf16[128,2048]{1,0:T(8,128)(2,1)}, bf16[128,2048]{1,0:T(8,128)(2,1)}, bf16[128,2048]{1,0:T(8,128)(2,1)}, f32[64,128]{1,0:T(8,128)}, bf16[128,1...) custom-call(bf16[128,2048]{1,0:T(8,128)(2,1)S(1)} %get-tuple-element.21.refs_0_, ...), custom_call_target="tpu_custom_call" | custom-call | tf_op jit(solution)/shard_map/pallas_call | solution.py:549

commit v3 on v2

--- a/solution.py
+++ b/solution.py
@@ -26,14 +26,18 @@
     ids_h, wts_h, mix_h, outg_h, gbr_h, st_h, dec_h, wp_h, wg_h, wu_h, wd_h,
     o_gate, o_up, o_down, o_proj, o_branch, o_drive, o_decay,
     ids, wts, mix, outg, gbr, st, dec, wp, wg, wu, wd,
-    onehot_s, disp, xc, acc_gu, acc_h, pbuf, precv, sbuf, rbuf, fin, ret, mid_all,
+    mixh, outh, onehot_s, weight_s, disp, near_send, xd, xc, acc_gu, acc_h, pbuf, precv, sbuf, rbuf, fin, ret, mid_all,
     gx_send, gx_recv, gz_send, gz_recv, car_send, car_recv, prev_b,
-    ins, s1, r1, rs, ds, rr, ps, pr, cs, cr, fs, fr, ms, mf, mr, xs, xr, zs, zr, ks, kr, vs, vr,
+    ins, s1, r1, n1, n2, nr, rs, ds, rr, ps, pr, cs, cr, fs, fr, ms, mf, mr, xs, xr, zs, zr, ks, kr, vs, vr,
 ):
     SP, X, TP, CAP = sizes
     Y = TP // 2
     H = Y // 2
+    Z = SP // X
+    near = near_blocks(SP, X)
+    far = SP - near
     SH = SP // 2
+    FH = far // 2
     n = mix_h.shape[0]
     d_model = mix_h.shape[1]
     slots = SP * CAP
@@ -45,8 +49,29 @@
     right = (t + 2) % TP
     left = (t + TP - 2) % TP
 
+    z = me // X
+    x = me % X
+
     def chip(off):
         return (y + off + Y) % Y
+
+    def moved(k, sign):
+        zi = k // X
+        dz = (zi + 1) // 2 * (2 * (zi % 2) - 1)
+        return (z + sign * dz + Z) % Z * X + (x + sign * (k % X) + X) % X
+
+    def target(k):
+        return moved(k, 1)
+
+    def source(k):
+        return moved(k, -1)
+
+    def each_block(lo, hi, body):
+        def step(k, carry):
+            body(k)
+            return carry
+
+        lax.fori_loop(lo, hi, step, 0)
 
     def remote(src, dst, send, recv, **device):
         return pltpu.make_async_remote_copy(
@@ -72,6 +97,8 @@
     pl.semaphore_signal(barrier, inc=1, device_id={"tp": partner}, device_id_type=MESH)
 
     own_cols = pl.ds(pl.multiple_of(t * LANES, LANES), LANES)
+    width = d_model // 2
+    half_cols = pl.ds(pl.multiple_of(core * width, width), width)
     fetch = [
         pltpu.make_async_copy(src, dst, ins.at[k])
         for k, (src, dst) in enumerate(
@@ -79,6 +106,7 @@
                 (ids_h, ids), (wts_h, wts), (mix_h.at[:, own_cols], mix),
                 (outg_h.at[:, own_cols], outg), (st_h, st), (wg_h, wg), (wu_h, wu), (wd_h, wd),
                 (gbr_h, gbr), (dec_h, dec), (wp_h, wp),
+                (mix_h.at[:, half_cols], mixh), (outg_h.at[:, half_cols], outh),
             )
         )
     ]
@@ -93,7 +121,12 @@
         lax.broadcasted_iota(jnp.int32, (n, n), 0) < lax.broadcasted_iota(jnp.int32, (n, n), 1)
     ).astype(F32).astype(BF16)
     before = dot((hots[0] + hots[1]).astype(BF16), earlier)
-    slot_io = lax.broadcasted_iota(jnp.int32, (slots, n), 0).astype(F32)
+    row = lax.broadcasted_iota(jnp.int32, (slots, n), 0)
+    kk = row >> (CAP.bit_length() - 1)
+    zi = kk >> (X.bit_length() - 1)
+    zz = (z + Z + ((zi + 1) >> 1) * (2 * (zi & 1) - 1)) & (Z - 1)
+    xx = (x + (kk & (X - 1))) & (X - 1)
+    slot_io = ((zz * X + xx) * CAP + (row & (CAP - 1))).astype(F32)
     picks = []
     for k in range(2):
         pos = jnp.sum(hots[k] * before, axis=0, keepdims=True)
@@ -104,19 +137,38 @@
         jnp.where(picks[0], wts[0:1, :], 0.0) + jnp.where(picks[1], wts[1:2, :], 0.0),
         axis=1, keepdims=True,
     )
-    x_slots = dot(onehot, mix[...]).astype(BF16)
-    c_slots = (weight * dot(onehot, outg[...])).astype(BF16)
-    disp[:, 0:CAP, :] = x_slots.reshape(SP, CAP, LANES)
-    disp[:, CAP : 2 * CAP, :] = c_slots.reshape(SP, CAP, LANES)
-    xc[t, me] = disp[me]
+    weight_s[...] = weight + jnp.zeros((slots, LANES), F32)
+    first = near * CAP
+
+    def into(ref, begin, lo, hi, mix_ref, out_ref):
+        pick = onehot_s[lo:hi, :]
+        shape = ((hi - lo) // CAP, CAP, mix_ref.shape[1])
+        end = begin + (hi - lo) // CAP
+        ref[begin:end, 0:CAP, :] = dot(pick, mix_ref[...]).astype(BF16).reshape(shape)
+        scaled = weight_s[lo:hi, 0:1] * dot(pick, out_ref[...])
+        ref[begin:end, CAP : 2 * CAP, :] = scaled.astype(BF16).reshape(shape)
+
+    into(disp, 0, first, slots, mix, outg)
 
     pl.semaphore_wait(barrier, SP - 1 + Y)
 
-    def dispatch(p):
-        return remote(disp.at[p], xc.at[t, me], s1.at[p], r1.at[me], sp=p)
-
-    each_peer(lambda p: dispatch(p).start())
-    for copy in fetch[4:]:
+    def dispatch(k):
+        return remote(disp.at[k], xc.at[t, k], s1.at[k], r1.at[k], sp=target(near + k))
+
+    def dispatch_near(k):
+        return remote(near_send.at[k], xd.at[core, k], n1.at[k], nr.at[core, k], sp=target(k))
+
+    def across_near(k, half):
+        return remote(xd.at[half, k], xd.at[half, k], n2.at[k], nr.at[half, k], tp=partner)
+
+    each_block(0, far, lambda k: dispatch(k).start())
+    for copy in fetch[11:]:
+        copy.wait()
+    into(near_send, 0, 0, first, mixh, outh)
+    each_block(1, near, lambda k: dispatch_near(k).start())
+    xd[core, 0] = near_send[0]
+    across_near(0, core).start()
+    for copy in fetch[4:11]:
         copy.wait()
     last_state = remote(
         st.at[pl.ds(n - 8, 8)], prev_b, vs.at[0], vr.at[0], sp=(me + 1) % SP
@@ -124,19 +176,10 @@
     last_state.start()
 
     def arrived_1(half):
-        def step(i, carry):
-            b = half * SH + i
-
-            @pl.when(b != me)
-            def _():
-                remote(disp.at[b], xc.at[t, b], s1.at[b], r1.at[b], sp=b).wait_recv()
-
-            return carry
-
-        lax.fori_loop(0, SH, step, 0)
+        each_block(half * FH, half * FH + FH, lambda k: dispatch(k).wait_recv())
 
     def half_of(src, h):
-        return xc.at[src, pl.ds(h * SH, SH)]
+        return xc.at[src, pl.ds(h * FH, FH)]
 
     def ring(src, h, way, step):
         dev = right if way == 0 else left
@@ -150,11 +193,27 @@
     acc_gu[...] = jnp.zeros_like(acc_gu)
     acc_h[...] = jnp.zeros_like(acc_h)
 
+    def span(part):
+        return (0, CAP) if part == 0 else (CAP, 2 * CAP)
+
     def pair_of(yy, part):
-        lo, hi = (0, CAP) if part == 0 else (CAP, 2 * CAP)
+        lo, hi = span(part)
         return jnp.concatenate(
-            [xc[2 * yy + k, :, lo:hi, :].reshape(slots, LANES) for k in range(2)], axis=1
-        )
+            [xc[2 * yy + k, :, lo:hi, :].reshape(far * CAP, LANES) for k in range(2)], axis=1
+        )
+
+    def near_rows(yy, part):
+        lo, hi = span(part)
+        at = yy % H * 2 * LANES
+        return xd[yy // H, :, lo:hi, at : at + 2 * LANES].reshape(first, 2 * LANES)
+
+    def forward_near(half):
+        cols = pl.ds(pl.multiple_of(half * width, width), width)
+        w_in = jnp.concatenate([wg[:, cols], wu[:, cols]], axis=0)
+        rows_x = xd[half, :, 0:CAP, :].reshape(first, width)
+        rows_c = xd[half, :, CAP : 2 * CAP, :].reshape(first, width)
+        acc_gu[0:first] += dot(rows_x, w_in, ((1,), (1,)))
+        acc_h[0:first] += dot(rows_c, wd[:, cols], ((1,), (1,)))
 
     def cols_of(yy):
         return pl.ds(pl.multiple_of(yy * 2 * LANES, 2 * LANES), 2 * LANES)
@@ -165,8 +224,8 @@
             across(other, h).wait_recv()
         cols = cols_of(yy)
         w_in = jnp.concatenate([wg[:, cols], wu[:, cols]], axis=0)
-        acc_gu[...] += dot(pair_of(yy, 0), w_in, ((1,), (1,)))
-        acc_h[...] += dot(pair_of(yy, 1), wd[:, cols], ((1,), (1,)))
+        acc_gu[first:slots] += dot(pair_of(yy, 0), w_in, ((1,), (1,)))
+        acc_h[first:slots] += dot(pair_of(yy, 1), wd[:, cols], ((1,), (1,)))
 
     for h in range(2):
         arrived_1(h)
@@ -184,9 +243,19 @@
             if s < most:
                 ring(src, h, way, s).start()
             across(src, h).start()
+        if s == H // 2:
+
+            def pass_near(k):
+                dispatch_near(k).wait_recv()
+                across_near(k, core).start()
+
+            each_block(1, near, pass_near)
         forward(chip(s - 1))
         if s > 1:
             forward(chip(1 - s))
+    forward_near(core)
+    each_block(0, near, lambda k: across_near(k, 1 - core).wait_recv())
+    forward_near(1 - core)
     forward(chip(H))
 
     gate = acc_gu[:, 0:LANES]
@@ -256,12 +325,15 @@
     grads_t = grads.T
     hidden_t = hidden.T
 
+    def all_rows(yy, part):
+        return jnp.concatenate([near_rows(yy, part), pair_of(yy, part)], axis=0)
+
     def weight_grads(yy):
         cols = cols_of(yy)
-        both = dot(grads_t, pair_of(yy, 0)).astype(BF16)
+        both = dot(grads_t, all_rows(yy, 0)).astype(BF16)
         o_gate[:, cols] = both[0:LANES]
         o_up[:, cols] = both[LANES : 2 * LANES]
-        o_down[:, cols] = dot(hidden_t, pair_of(yy, 1)).astype(BF16)
+        o_down[:, cols] = dot(hidden_t, all_rows(yy, 1)).astype(BF16)
 
     todo = list(range(Y))
     per_step = -(-Y // H)
@@ -280,8 +352,8 @@
     while todo:
         weight_grads(todo.pop(0))
 
-    def give(p):
-        return remote(fin.at[p], ret.at[me], fs.at[p], fr.at[me], sp=p)
+    def give(k):
+        return remote(fin.at[k], ret.at[k], fs.at[k], fr.at[k], sp=source(k))
 
     for h in range(2):
         total = own_sum(0, h)
@@ -291,17 +363,8 @@
             total = total + rbuf[way, h, step].astype(F32)
         fin[pl.ds(h * SH, SH)] = total.astype(BF16).reshape(SH, CAP, LANES)
 
-        def send_back(i, carry):
-            b = h * SH + i
-
-            @pl.when(b != me)
-            def _():
-                give(b).start()
-
-            return carry
-
-        lax.fori_loop(0, SH, send_back, 0)
-    ret[me] = fin[me]
+        each_block(max(1, h * SH), (h + 1) * SH, lambda k: give(k).start())
+    ret[0] = fin[0]
 
     onehot_t = onehot_s[...].T
     out_cols = outg[...].astype(F32)
@@ -313,7 +376,7 @@
         prods.append(prod)
         prod = prod * shift_up(prod, k, 1.0)
 
-    each_peer(lambda p: remote(fin.at[p], ret.at[p], fs.at[p], fr.at[p], sp=p).wait_recv())
+    each_block(1, SP, lambda k: give(k).wait_recv())
     routed = dot(onehot_t, ret[...].reshape(slots, LANES))
     mid_all[t] = (out_cols + routed).astype(BF16)
 
@@ -331,8 +394,6 @@
         share(off % Y).start()
 
     block = d_model // SP
-    z = me // X
-    x = me % X
 
     def over_x(yy, j):
         return remote(
@@ -416,8 +477,8 @@
     drive = grad + prod * entering
     o_drive[...] = drive
     last_state.wait_recv()
-    first = jnp.where(me > 0, 1.0, 0.0) * prev_b[7:8, :]
-    o_decay[...] = drive * jnp.concatenate([first, states[: n - 1]], axis=0)
+    prior = jnp.where(me > 0, 1.0, 0.0) * prev_b[7:8, :]
+    o_decay[...] = drive * jnp.concatenate([prior, states[: n - 1]], axis=0)
 
     def z_peers(body):
         def step(i, carry):
@@ -437,11 +498,13 @@
     o_proj[...] = total
 
     def drain(p):
-        dispatch(p).wait_send()
-        give(p).wait_send()
         carry_to(p).wait_send()
 
     each_peer(drain)
+    each_block(0, far, lambda k: dispatch(k).wait_send())
+    each_block(1, near, lambda k: dispatch_near(k).wait_send())
+    each_block(0, near, lambda k: across_near(k, core).wait_send())
+    each_block(1, SP, lambda k: give(k).wait_send())
     last_state.wait_send()
     z_peers(lambda p: over_z(p).wait_send())
     for yy in range(Y):
@@ -461,6 +524,10 @@
         share(off).wait_send()
 
 
+def near_blocks(SP, X):
+    return 3 * X
+
+
 def store(*refs):
     count = len(refs) // 2
     copies = [
@@ -483,6 +550,8 @@
     CAP = min(n, 2 * route_ids.shape[1] * n // SP)
     slots = SP * CAP
     X = SP // Y
+    near = near_blocks(SP, X)
+    far = SP - near
     block = d_model // SP
     dma = pltpu.SemaphoreType.DMA
     big = jax.ShapeDtypeStruct((LANES, d_model), BF16)
@@ -510,9 +579,14 @@
             pltpu.VMEM((LANES, d_model), BF16),
             pltpu.VMEM((LANES, d_model), BF16),
             pltpu.VMEM((LANES, d_model), BF16),
+            pltpu.VMEM((n, d_model // 2), BF16),
+            pltpu.VMEM((n, d_model // 2), BF16),
             pltpu.VMEM((slots, n), BF16),
-            pltpu.VMEM((SP, 2 * CAP, LANES), BF16),
-            pltpu.VMEM((TP, SP, 2 * CAP, LANES), BF16),
+            pltpu.VMEM((slots, LANES), F32),
+            pltpu.VMEM((far, 2 * CAP, LANES), BF16),
+            pltpu.VMEM((near, 2 * CAP, d_model // 2), BF16),
+            pltpu.VMEM((2, near, 2 * CAP, d_model // 2), BF16),
+            pltpu.VMEM((TP, far, 2 * CAP, LANES), BF16),
             pltpu.VMEM((slots, 2 * LANES), F32),
             pltpu.VMEM((slots, LANES), F32),
             pltpu.VMEM((Y, 2, slots, LANES), BF16),
@@ -529,7 +603,7 @@
             pltpu.VMEM((2, LANES), F32),
             pltpu.VMEM((SP, 2, LANES), F32),
             pltpu.VMEM((8, LANES), F32),
-            dma((11,)), dma((SP,)), dma((SP,)),
+            dma((13,)), dma((far,)), dma((far,)), dma((near,)), dma((near,)), dma((2, near)),
             dma((2, 2, H)), dma((Y, 2)), dma((TP, 2)),
             dma((Y,)), dma((Y,)),
             dma((2, 2, H)), dma((2, 2, H)),

time: 98.8 us -> 95 us (0.962)
  Pallas kernels: 97.6 us -> 94.2 us
    pallas_call x1, Pallas kernels: 96.4 us -> 93 us  [local(): pl.pallas_call(functools.partial(kernel, (SP, SP // Y, TP, CAP)), out_sha...]
where the time goes in v3:
time: 95 us; the launch traced here: 94.9 us
  Pallas kernels  94.2 us (99%)
    pallas_call x1, Pallas kernels, local(): pl.pallas_call(functools.partial(kernel, (SP, SP // Y, TP, CAP)), out_sha...  93 us

profile of v3, /device:TPU:1, one launch (start us, length us, event | category | flops | bytes accessed | tf_op | source)
XLA Modules:
  0.0 94.9 jit_solution(11775447908522456989)
XLA Ops:
  0.6 93.0 %shard_map.162 = (bf16[128,2048]{1,0:T(8,128)(2,1)S(1)}, bf16[128,2048]{1,0:T(8,128)(2,1)S(1)}, bf16[128,2048]{1,0:T(8,128)(2,1)S(1)}, f32[64,128]{1,0:T(8,128)S...) custom-call(s32[2,128]{1,0:T(2,128)} %bitcast.11, f32[2,128]{1,0:T(2,128)} %bitcast.12, ...), custom_call_target="tpu_custom_call" | custom-call | tf_op jit(solution)/shard_map/pallas_call | solution.py:559
  93.6 1.3 %shard_map.163 = (bf16[128,2048]{1,0:T(8,128)(2,1)}, bf16[128,2048]{1,0:T(8,128)(2,1)}, bf16[128,2048]{1,0:T(8,128)(2,1)}, f32[64,128]{1,0:T(8,128)}, bf16[128,1...) custom-call(bf16[128,2048]{1,0:T(8,128)(2,1)S(1)} %get-tuple-element.21.refs_0_, ...), custom_call_target="tpu_custom_call" | custom-call | tf_op jit(solution)/shard_map/pallas_call | solution.py:623

commit v4 on v3

--- a/solution.py
+++ b/solution.py
@@ -36,8 +36,8 @@
     Z = SP // X
     near = near_blocks(SP, X)
     far = SP - near
-    SH = SP // 2
-    FH = far // 2
+    groups = ring_groups(far, X)
+    quarter = SP // 4
     n = mix_h.shape[0]
     d_model = mix_h.shape[1]
     slots = SP * CAP
@@ -165,7 +165,6 @@
     for copy in fetch[11:]:
         copy.wait()
     into(near_send, 0, 0, first, mixh, outh)
-    each_block(1, near, lambda k: dispatch_near(k).start())
     xd[core, 0] = near_send[0]
     across_near(0, core).start()
     for copy in fetch[4:11]:
@@ -175,11 +174,12 @@
     )
     last_state.start()
 
-    def arrived_1(half):
-        each_block(half * FH, half * FH + FH, lambda k: dispatch(k).wait_recv())
+    def arrived_1(g):
+        lo, count = groups[g]
+        each_block(lo, lo + count, lambda k: dispatch(k).wait_recv())
 
     def half_of(src, h):
-        return xc.at[src, pl.ds(h * FH, FH)]
+        return xc.at[src, pl.ds(groups[h][0], groups[h][1])]
 
     def ring(src, h, way, step):
         dev = right if way == 0 else left
@@ -220,40 +220,53 @@
 
     def forward(yy):
         other = 2 * yy + 1 - core
-        for h in range(2):
+        for h in range(len(groups)):
             across(other, h).wait_recv()
         cols = cols_of(yy)
         w_in = jnp.concatenate([wg[:, cols], wu[:, cols]], axis=0)
         acc_gu[first:slots] += dot(pair_of(yy, 0), w_in, ((1,), (1,)))
         acc_h[first:slots] += dot(pair_of(yy, 1), wd[:, cols], ((1,), (1,)))
 
-    for h in range(2):
-        arrived_1(h)
-        for way in range(2):
-            ring(t, h, way, 0).start()
-        across(t, h).start()
-
-    for s in range(1, H + 1):
-        for way, h in ((0, 0), (1, 1), (1, 0), (0, 1)):
-            most = H if way == h else H - 1
-            if s > most:
+    def reach(way, h):
+        return H if way == h % 2 else H - 1
+
+    begins = [0.0, 0.0, 3.5, 4.2, 5.0, 5.9][: len(groups)]
+    events = sorted(
+        (begins[h] + 4.4 * step, step, h) for h in range(len(groups)) for step in range(H + 1)
+    )
+    last_of = {step: max(e for e in events if e[1] == step) for step in range(H + 1)}
+    for event in events:
+        _, step, h = event
+        if step == 0:
+            arrived_1(h)
+            for way in range(2):
+                ring(t, h, way, 0).start()
+            across(t, h).start()
+        for way in range(2) if step else ():
+            most = reach(way, h)
+            if step > most:
                 continue
-            src = 2 * chip(-s if way == 0 else s) + core
-            ring(src, h, way, s - 1).wait_recv()
-            if s < most:
-                ring(src, h, way, s).start()
+            src = 2 * chip(-step if way == 0 else step) + core
+            ring(src, h, way, step - 1).wait_recv()
+            if step < most:
+                ring(src, h, way, step).start()
             across(src, h).start()
-        if s == H // 2:
+        if event != last_of[step]:
+            continue
+        if step == 0:
+            each_block(1, near, lambda k: dispatch_near(k).start())
+            continue
+        if step == H - 1:
 
             def pass_near(k):
                 dispatch_near(k).wait_recv()
                 across_near(k, core).start()
 
             each_block(1, near, pass_near)
-        forward(chip(s - 1))
-        if s > 1:
-            forward(chip(1 - s))
-    forward_near(core)
+            forward_near(core)
+        forward(chip(step - 1))
+        if step > 1:
+            forward(chip(1 - step))
     each_block(0, near, lambda k: across_near(k, 1 - core).wait_recv())
     forward_near(1 - core)
     forward(chip(H))
@@ -279,7 +292,7 @@
     def swap(yy):
         return remote(pbuf.at[yy, 1 - core], precv.at[yy], ps.at[yy], pr.at[yy], tp=partner)
 
-    rows = slots // 2
+    rows = slots // 4
 
     def own_sum(off, h):
         yy = chip(off)
@@ -293,10 +306,10 @@
             cs.at[way, h, step], cr.at[way, h, step], tp=dev,
         )
 
-    flows = ((0, 0), (1, 1), (0, 1), (1, 0))
+    flows = ((1, 2), (1, 3), (0, 0), (0, 1), (0, 2), (0, 3), (1, 0), (1, 1))
 
     def length(way, h):
-        return H if way == h else H - 1
+        return H if way == h // 2 else H - 1
 
     def sign(way):
         return 1 if way == 0 else -1
@@ -305,12 +318,13 @@
     partial(H - 1)
     partial(1 - H)
     swap(chip(H)).wait_recv()
-    for way, h in flows[:2]:
+    for way, h in flows[:4]:
         sbuf[way, h, 0] = own_sum(H, h).astype(BF16)
         chain(way, h, 0).start()
-    for way, h in flows[2:]:
+    for way, h in flows[4:]:
         off = sign(way) * (H - 1)
-        swap(chip(off)).wait_recv()
+        if h % 2 == 0:
+            swap(chip(off)).wait_recv()
         sbuf[way, h, 0] = own_sum(off, h).astype(BF16)
         chain(way, h, 0).start()
     for m in range(H - 2, 0, -1):
@@ -355,15 +369,15 @@
     def give(k):
         return remote(fin.at[k], ret.at[k], fs.at[k], fr.at[k], sp=source(k))
 
-    for h in range(2):
+    for h in (2, 3, 0, 1):
         total = own_sum(0, h)
         for way in range(2):
             step = length(way, h) - 1
             chain(way, h, step).wait_recv()
             total = total + rbuf[way, h, step].astype(F32)
-        fin[pl.ds(h * SH, SH)] = total.astype(BF16).reshape(SH, CAP, LANES)
-
-        each_block(max(1, h * SH), (h + 1) * SH, lambda k: give(k).start())
+        fin[pl.ds(h * quarter, quarter)] = total.astype(BF16).reshape(quarter, CAP, LANES)
+
+        each_block(max(1, h * quarter), (h + 1) * quarter, lambda k: give(k).start())
     ret[0] = fin[0]
 
     onehot_t = onehot_s[...].T
@@ -390,7 +404,7 @@
 
     order = [off for m in range(1, H) for off in (m, -m)] + [H]
     pass_mid(t).start()
-    for off in order[::-1]:
+    for off in order:
         share(off % Y).start()
 
     block = d_model // SP
@@ -446,7 +460,8 @@
             forward_proj(chip(behind.pop(0)))
     for off in queue:
         act = act + project(chip(off))
-        behind.append(off)
+    for off in behind:
+        forward_proj(chip(off))
 
     states = st[...]
     o_branch[...] = (act * states).astype(BF16)
@@ -462,7 +477,7 @@
         return remote(car_send, car_recv.at[me], ks.at[p], kr.at[me], sp=p)
 
     each_peer(lambda p: carry_to(p).start())
-    for off in behind:
+    for off in queue:
         forward_proj(chip(off))
     car_recv[me] = car_send[...]
     each_peer(lambda p: remote(car_send, car_recv.at[p], ks.at[p], kr.at[p], sp=p).wait_recv())
@@ -510,13 +525,14 @@
     for yy in range(Y):
         x_peers(lambda j: over_x(yy, j).wait_send())
     for way in range(2):
-        for h in range(2):
-            most = length(way, h)
-            for s in range(most):
-                ring(t, h, way, s).wait_send()
-                chain(way, h, s).wait_send()
+        for h in range(len(groups)):
+            for step in range(reach(way, h)):
+                ring(t, h, way, step).wait_send()
+        for h in range(4):
+            for step in range(length(way, h)):
+                chain(way, h, step).wait_send()
     for yy in range(Y):
-        for h in range(2):
+        for h in range(len(groups)):
             across(2 * yy + core, h).wait_send()
         swap(yy).wait_send()
         pass_mid(2 * yy + core).wait_send()
@@ -525,7 +541,14 @@
 
 
 def near_blocks(SP, X):
-    return 3 * X
+    return X
+
+
+def ring_groups(far, X):
+    rest = far - 2 * X
+    parts = min(4, rest)
+    sizes = [X, X] + [rest * (k + 1) // parts - rest * k // parts for k in range(parts)]
+    return [(sum(sizes[:k]), sizes[k]) for k in range(len(sizes))]
 
 
 def store(*refs):
@@ -552,6 +575,7 @@
     X = SP // Y
     near = near_blocks(SP, X)
     far = SP - near
+    pieces = len(ring_groups(far, X))
     block = d_model // SP
     dma = pltpu.SemaphoreType.DMA
     big = jax.ShapeDtypeStruct((LANES, d_model), BF16)
@@ -591,8 +615,8 @@
             pltpu.VMEM((slots, LANES), F32),
             pltpu.VMEM((Y, 2, slots, LANES), BF16),
             pltpu.VMEM((Y, slots, LANES), BF16),
-            pltpu.VMEM((2, 2, H, slots // 2, LANES), BF16),
-            pltpu.VMEM((2, 2, H, slots // 2, LANES), BF16),
+            pltpu.VMEM((2, 4, H, slots // 4, LANES), BF16),
+            pltpu.VMEM((2, 4, H, slots // 4, LANES), BF16),
             pltpu.VMEM((SP, CAP, LANES), BF16),
             pltpu.VMEM((SP, CAP, LANES), BF16),
             pltpu.VMEM((TP, n, LANES), BF16),
@@ -604,9 +628,9 @@
             pltpu.VMEM((SP, 2, LANES), F32),
             pltpu.VMEM((8, LANES), F32),
             dma((13,)), dma((far,)), dma((far,)), dma((near,)), dma((near,)), dma((2, near)),
-            dma((2, 2, H)), dma((Y, 2)), dma((TP, 2)),
+            dma((2, pieces, H)), dma((Y, pieces)), dma((TP, pieces)),
             dma((Y,)), dma((Y,)),
-            dma((2, 2, H)), dma((2, 2, H)),
+            dma((2, 4, H)), dma((2, 4, H)),
             dma((SP,)), dma((SP,)),
             dma((Y,)), dma((Y,)), dma((TP,)),
             dma((Y, X)), dma((Y, X)), dma((Y,)), dma((Y,)),

time: 95 us -> 94.7 us (level)
  no operation moved by 1% of the time
where the time goes in v4:
time: 94.7 us; the launch traced here: 94 us
  Pallas kernels  93.4 us (99%)
    pallas_call x1, Pallas kernels, local(): pl.pallas_call(functools.partial(kernel, (SP, SP // Y, TP, CAP)), out_sha...  92.1 us

profile of v4, /device:TPU:1, one launch (start us, length us, event | category | flops | bytes accessed | tf_op | source)
XLA Modules:
  0.0 94.0 jit_solution(15628794855991942490)
XLA Ops:
  0.6 92.1 %shard_map.162 = (bf16[128,2048]{1,0:T(8,128)(2,1)S(1)}, bf16[128,2048]{1,0:T(8,128)(2,1)S(1)}, bf16[128,2048]{1,0:T(8,128)(2,1)S(1)}, f32[64,128]{1,0:T(8,128)S...) custom-call(s32[2,128]{1,0:T(2,128)} %bitcast.11, f32[2,128]{1,0:T(2,128)} %bitcast.12, ...), custom_call_target="tpu_custom_call" | custom-call | tf_op jit(solution)/shard_map/pallas_call | solution.py:583
  92.8 1.3 %shard_map.163 = (bf16[128,2048]{1,0:T(8,128)(2,1)}, bf16[128,2048]{1,0:T(8,128)(2,1)}, bf16[128,2048]{1,0:T(8,128)(2,1)}, f32[64,128]{1,0:T(8,128)}, bf16[128,1...) custom-call(bf16[128,2048]{1,0:T(8,128)(2,1)S(1)} %get-tuple-element.21.refs_0_, ...), custom_call_target="tpu_custom_call" | custom-call | tf_op jit(solution)/shard_map/pallas_call | solution.py:647

commit v5 on v4

--- a/solution.py
+++ b/solution.py
@@ -36,7 +36,7 @@
     Z = SP // X
     near = near_blocks(SP, X)
     far = SP - near
-    groups = ring_groups(far, X)
+    groups = ring_groups(far)
     quarter = SP // 4
     n = mix_h.shape[0]
     d_model = mix_h.shape[1]
@@ -161,7 +161,7 @@
     def across_near(k, half):
         return remote(xd.at[half, k], xd.at[half, k], n2.at[k], nr.at[half, k], tp=partner)
 
-    each_block(0, far, lambda k: dispatch(k).start())
+    each_block(0, far, lambda k: dispatch(far - 1 - k).start())
     for copy in fetch[11:]:
         copy.wait()
     into(near_send, 0, 0, first, mixh, outh)
@@ -230,13 +230,14 @@
     def reach(way, h):
         return H if way == h % 2 else H - 1
 
-    begins = [0.0, 0.0, 3.5, 4.2, 5.0, 5.9][: len(groups)]
-    events = sorted(
-        (begins[h] + 4.4 * step, step, h) for h in range(len(groups)) for step in range(H + 1)
-    )
-    last_of = {step: max(e for e in events if e[1] == step) for step in range(H + 1)}
+    events = [(step, h) for step in range(H + 1) for h in range(len(groups))[::-1]]
+    def other_near():
+        each_block(0, near, lambda k: across_near(k, 1 - core).wait_recv())
+        forward_near(1 - core)
+
+    late = [lambda: forward(chip(H - 1)), lambda: forward(chip(1 - H)), other_near]
     for event in events:
-        _, step, h = event
+        step, h = event
         if step == 0:
             arrived_1(h)
             for way in range(2):
@@ -251,11 +252,18 @@
             if step < most:
                 ring(src, h, way, step).start()
             across(src, h).start()
-        if event != last_of[step]:
+        if step == H and late:
+            late.pop(0)()
+        if h:
             continue
         if step == 0:
             each_block(1, near, lambda k: dispatch_near(k).start())
             continue
+        if step == H:
+            continue
+        forward(chip(step - 1))
+        if step > 1:
+            forward(chip(1 - step))
         if step == H - 1:
 
             def pass_near(k):
@@ -264,11 +272,8 @@
 
             each_block(1, near, pass_near)
             forward_near(core)
-        forward(chip(step - 1))
-        if step > 1:
-            forward(chip(1 - step))
-    each_block(0, near, lambda k: across_near(k, 1 - core).wait_recv())
-    forward_near(1 - core)
+    for job in late:
+        job()
     forward(chip(H))
 
     gate = acc_gu[:, 0:LANES]
@@ -367,7 +372,7 @@
         weight_grads(todo.pop(0))
 
     def give(k):
-        return remote(fin.at[k], ret.at[k], fs.at[k], fr.at[k], sp=source(k))
+        return remote(fin.at[k], ret.at[k], fs.at[0], fr.at[0], sp=source(k))
 
     for h in (2, 3, 0, 1):
         total = own_sum(0, h)
@@ -390,7 +395,24 @@
         prods.append(prod)
         prod = prod * shift_up(prod, k, 1.0)
 
-    each_block(1, SP, lambda k: give(k).wait_recv())
+    each_block(0, far, lambda k: dispatch(k).wait_send())
+    each_block(1, near, lambda k: dispatch_near(k).wait_send())
+    each_block(0, near, lambda k: across_near(k, core).wait_send())
+    last_state.wait()
+    for way in range(2):
+        for h in range(len(groups)):
+            for step in range(reach(way, h)):
+                ring(t, h, way, step).wait_send()
+        for h in range(4):
+            for step in range(length(way, h)):
+                chain(way, h, step).wait_send()
+    for yy in range(Y):
+        for h in range(len(groups)):
+            across(2 * yy + core, h).wait_send()
+        swap(yy).wait_send()
+    rest = pl.ds(1, SP - 1)
+    given = remote(fin.at[rest], ret.at[rest], fs.at[0], fr.at[0], sp=source(1))
+    given.wait_recv()
     routed = dot(onehot_t, ret[...].reshape(slots, LANES))
     mid_all[t] = (out_cols + routed).astype(BF16)
 
@@ -460,8 +482,6 @@
             forward_proj(chip(behind.pop(0)))
     for off in queue:
         act = act + project(chip(off))
-    for off in behind:
-        forward_proj(chip(off))
 
     states = st[...]
     o_branch[...] = (act * states).astype(BF16)
@@ -474,13 +494,21 @@
     car_send[1:2, :] = head * grad[0:1, :]
 
     def carry_to(p):
-        return remote(car_send, car_recv.at[me], ks.at[p], kr.at[me], sp=p)
+        return remote(car_send, car_recv.at[me], ks.at[0], kr.at[0], sp=p)
 
     each_peer(lambda p: carry_to(p).start())
-    for off in queue:
+    for off in behind + queue:
         forward_proj(chip(off))
     car_recv[me] = car_send[...]
-    each_peer(lambda p: remote(car_send, car_recv.at[p], ks.at[p], kr.at[p], sp=p).wait_recv())
+    given.wait_send()
+    for off in range(1, Y):
+        share(off).wait_send()
+    for yy in range(Y):
+        pass_mid(2 * yy + core).wait_send()
+        x_peers(lambda j: over_x(yy, j).wait_send())
+    others = car_recv.at[pl.ds(0, SP - 1)]
+    sent_carry = remote(others, others, ks.at[0], kr.at[0], sp=(me + 1) % SP)
+    sent_carry.wait_recv()
 
     def enter(i, value):
         b = SP - 1 - i
@@ -491,7 +519,6 @@
     entering = lax.fori_loop(0, SP - 1, enter, jnp.zeros((1, LANES), F32))
     drive = grad + prod * entering
     o_drive[...] = drive
-    last_state.wait_recv()
     prior = jnp.where(me > 0, 1.0, 0.0) * prev_b[7:8, :]
     o_decay[...] = drive * jnp.concatenate([prior, states[: n - 1]], axis=0)
 
@@ -512,43 +539,18 @@
         total = total + gz_recv[(z + i) % Y].astype(F32)
     o_proj[...] = total
 
-    def drain(p):
-        carry_to(p).wait_send()
-
-    each_peer(drain)
-    each_block(0, far, lambda k: dispatch(k).wait_send())
-    each_block(1, near, lambda k: dispatch_near(k).wait_send())
-    each_block(0, near, lambda k: across_near(k, core).wait_send())
-    each_block(1, SP, lambda k: give(k).wait_send())
-    last_state.wait_send()
+    sent_carry.wait_send()
     z_peers(lambda p: over_z(p).wait_send())
-    for yy in range(Y):
-        x_peers(lambda j: over_x(yy, j).wait_send())
-    for way in range(2):
-        for h in range(len(groups)):
-            for step in range(reach(way, h)):
-                ring(t, h, way, step).wait_send()
-        for h in range(4):
-            for step in range(length(way, h)):
-                chain(way, h, step).wait_send()
-    for yy in range(Y):
-        for h in range(len(groups)):
-            across(2 * yy + core, h).wait_send()
-        swap(yy).wait_send()
-        pass_mid(2 * yy + core).wait_send()
-    for off in range(1, Y):
-        share(off).wait_send()
 
 
 def near_blocks(SP, X):
-    return X
-
-
-def ring_groups(far, X):
-    rest = far - 2 * X
-    parts = min(4, rest)
-    sizes = [X, X] + [rest * (k + 1) // parts - rest * k // parts for k in range(parts)]
-    return [(sum(sizes[:k]), sizes[k]) for k in range(len(sizes))]
+    return 3 * X
+
+
+def ring_groups(far):
+    parts = min(4, far)
+    cuts = [far * k // parts for k in range(parts + 1)]
+    return [(lo, hi - lo) for lo, hi in zip(cuts, cuts[1:])]
 
 
 def store(*refs):
@@ -575,7 +577,7 @@
     X = SP // Y
     near = near_blocks(SP, X)
     far = SP - near
-    pieces = len(ring_groups(far, X))
+    pieces = len(ring_groups(far))
     block = d_model // SP
     dma = pltpu.SemaphoreType.DMA
     big = jax.ShapeDtypeStruct((LANES, d_model), BF16)
@@ -631,10 +633,10 @@
             dma((2, pieces, H)), dma((Y, pieces)), dma((TP, pieces)),
             dma((Y,)), dma((Y,)),
             dma((2, 4, H)), dma((2, 4, H)),
-            dma((SP,)), dma((SP,)),
+            dma((1,)), dma((1,)),
             dma((Y,)), dma((Y,)), dma((TP,)),
             dma((Y, X)), dma((Y, X)), dma((Y,)), dma((Y,)),
-            dma((SP,)), dma((SP,)),
+            dma((1,)), dma((1,)),
             dma((1,)), dma((1,)),
         ],
         compiler_params=pltpu.CompilerParams(

time: 94.7 us -> 86.6 us (0.914)
  Pallas kernels: 93.4 us -> 85.9 us
    pallas_call x1, Pallas kernels: 92.1 us -> 84.6 us  [local(): pl.pallas_call(functools.partial(kernel, (SP, SP // Y, TP, CAP)), out_sha...]
where the time goes in v5:
time: 86.6 us; the launch traced here: 86.5 us
  Pallas kernels  85.9 us (99%)
    pallas_call x1, Pallas kernels, local(): pl.pallas_call(functools.partial(kernel, (SP, SP // Y, TP, CAP)), out_sha...  84.6 us

profile of v5, /device:TPU:1, one launch (start us, length us, event | category | flops | bytes accessed | tf_op | source)
XLA Modules:
  0.0 86.5 jit_solution(11308598728670804264)
XLA Ops:
  0.6 84.6 %shard_map.162 = (bf16[128,2048]{1,0:T(8,128)(2,1)S(1)}, bf16[128,2048]{1,0:T(8,128)(2,1)S(1)}, bf16[128,2048]{1,0:T(8,128)(2,1)S(1)}, f32[64,128]{1,0:T(8,128)S...) custom-call(s32[2,128]{1,0:T(2,128)} %bitcast.11, f32[2,128]{1,0:T(2,128)} %bitcast.12, ...), custom_call_target="tpu_custom_call" | custom-call | tf_op jit(solution)/shard_map/pallas_call | solution.py:585
  85.2 1.3 %shard_map.163 = (bf16[128,2048]{1,0:T(8,128)(2,1)}, bf16[128,2048]{1,0:T(8,128)(2,1)}, bf16[128,2048]{1,0:T(8,128)(2,1)}, f32[64,128]{1,0:T(8,128)}, bf16[128,1...) custom-call(bf16[128,2048]{1,0:T(8,128)(2,1)S(1)} %get-tuple-element.21.refs_0_, ...), custom_call_target="tpu_custom_call" | custom-call | tf_op jit(solution)/shard_map/pallas_call | solution.py:649

commit v6 on v5

--- a/solution.py
+++ b/solution.py
@@ -46,14 +46,21 @@
     y = t // 2
     core = t % 2
     partner = t + 1 - 2 * core
-    right = (t + 2) % TP
-    left = (t + TP - 2) % TP
 
     z = me // X
     x = me % X
 
     def chip(off):
         return (y + off + Y) % Y
+
+    def other_core(off):
+        return 2 * chip(off) + 1 - core
+
+    right = other_core(1)
+    left = other_core(-1)
+
+    def lane(off):
+        return core if off % 2 == 0 else 1 - core
 
     def moved(k, sign):
         zi = k // X
@@ -73,28 +80,14 @@
 
         lax.fori_loop(lo, hi, step, 0)
 
+    def each_peer(body):
+        each_block(0, SP - 1, lambda i: body(target(SP - 1 - i)))
+
     def remote(src, dst, send, recv, **device):
         return pltpu.make_async_remote_copy(
             src_ref=src, dst_ref=dst, send_sem=send, recv_sem=recv,
             device_id=device, device_id_type=MESH,
         )
-
-    def each_peer(body):
-        def step(i, carry):
-            body((me + 1 + i) % SP)
-            return carry
-
-        lax.fori_loop(0, SP - 1, step, 0)
-
-    barrier = pltpu.get_barrier_semaphore()
-    each_peer(
-        lambda p: pl.semaphore_signal(barrier, inc=1, device_id={"sp": p}, device_id_type=MESH)
-    )
-    for off in range(1, Y):
-        pl.semaphore_signal(
-            barrier, inc=1, device_id={"tp": (t + 2 * off) % TP}, device_id_type=MESH
-        )
-    pl.semaphore_signal(barrier, inc=1, device_id={"tp": partner}, device_id_type=MESH)
 
     own_cols = pl.ds(pl.multiple_of(t * LANES, LANES), LANES)
     width = d_model // 2
@@ -112,6 +105,17 @@
     ]
     for copy in fetch:
         copy.start()
+
+    barrier = pltpu.get_barrier_semaphore()
+    each_peer(
+        lambda p: pl.semaphore_signal(barrier, inc=1, device_id={"sp": p}, device_id_type=MESH)
+    )
+    for off in range(1, Y):
+        pl.semaphore_signal(
+            barrier, inc=1, device_id={"tp": other_core(off)}, device_id_type=MESH
+        )
+    pl.semaphore_signal(barrier, inc=1, device_id={"tp": partner}, device_id_type=MESH)
+
     for copy in fetch[:4]:
         copy.wait()
 
@@ -218,8 +222,9 @@
     def cols_of(yy):
         return pl.ds(pl.multiple_of(yy * 2 * LANES, 2 * LANES), 2 * LANES)
 
-    def forward(yy):
-        other = 2 * yy + 1 - core
+    def forward(off):
+        yy = chip(off)
+        other = 2 * yy + 1 - lane(off)
         for h in range(len(groups)):
             across(other, h).wait_recv()
         cols = cols_of(yy)
@@ -235,7 +240,7 @@
         each_block(0, near, lambda k: across_near(k, 1 - core).wait_recv())
         forward_near(1 - core)
 
-    late = [lambda: forward(chip(H - 1)), lambda: forward(chip(1 - H)), other_near]
+    late = [lambda: forward(H - 1), lambda: forward(1 - H), other_near]
     for event in events:
         step, h = event
         if step == 0:
@@ -247,7 +252,7 @@
             most = reach(way, h)
             if step > most:
                 continue
-            src = 2 * chip(-step if way == 0 else step) + core
+            src = 2 * chip(-step if way == 0 else step) + lane(step)
             ring(src, h, way, step - 1).wait_recv()
             if step < most:
                 ring(src, h, way, step).start()
@@ -261,9 +266,9 @@
             continue
         if step == H:
             continue
-        forward(chip(step - 1))
+        forward(step - 1)
         if step > 1:
-            forward(chip(1 - step))
+            forward(1 - step)
         if step == H - 1:
 
             def pass_near(k):
@@ -274,7 +279,7 @@
             forward_near(core)
     for job in late:
         job()
-    forward(chip(H))
+    forward(H)
 
     gate = acc_gu[:, 0:LANES]
     up = acc_gu[:, LANES : 2 * LANES]
@@ -292,17 +297,18 @@
         value = dot(grads, jnp.concatenate([wg[:, cols], wu[:, cols]], axis=0)).astype(BF16)
         pbuf[yy, 0] = value[:, 0:LANES]
         pbuf[yy, 1] = value[:, LANES : 2 * LANES]
-        swap(yy).start()
-
-    def swap(yy):
-        return remote(pbuf.at[yy, 1 - core], precv.at[yy], ps.at[yy], pr.at[yy], tp=partner)
+        swap(off).start()
+
+    def swap(off):
+        yy = chip(off)
+        return remote(pbuf.at[yy, 1 - lane(off)], precv.at[yy], ps.at[yy], pr.at[yy], tp=partner)
 
     rows = slots // 4
 
     def own_sum(off, h):
         yy = chip(off)
         part = pl.ds(h * rows, rows)
-        return pbuf[yy, core, part, :].astype(F32) + precv[yy, part, :].astype(F32)
+        return pbuf[yy, lane(off), part, :].astype(F32) + precv[yy, part, :].astype(F32)
 
     def chain(way, h, step):
         dev = right if way == 0 else left
@@ -322,14 +328,14 @@
     partial(H)
     partial(H - 1)
     partial(1 - H)
-    swap(chip(H)).wait_recv()
+    swap(H).wait_recv()
     for way, h in flows[:4]:
         sbuf[way, h, 0] = own_sum(H, h).astype(BF16)
         chain(way, h, 0).start()
     for way, h in flows[4:]:
         off = sign(way) * (H - 1)
         if h % 2 == 0:
-            swap(chip(off)).wait_recv()
+            swap(off).wait_recv()
         sbuf[way, h, 0] = own_sum(off, h).astype(BF16)
         chain(way, h, 0).start()
     for m in range(H - 2, 0, -1):
@@ -337,9 +343,9 @@
         partial(-m)
     partial(0)
     for m in range(H - 2, 0, -1):
-        swap(chip(m)).wait_recv()
-        swap(chip(-m)).wait_recv()
-    swap(chip(0)).wait_recv()
+        swap(m).wait_recv()
+        swap(-m).wait_recv()
+    swap(0).wait_recv()
 
     grads_t = grads.T
     hidden_t = hidden.T
@@ -418,7 +424,7 @@
 
     def share(off):
         return remote(
-            mid_all.at[t], mid_all.at[t], ms.at[off], mr.at[t], tp=(t + 2 * off) % TP
+            mid_all.at[t], mid_all.at[t], ms.at[off], mr.at[t], tp=other_core(off)
         )
 
     def pass_mid(src):
@@ -443,8 +449,9 @@
         for j in range(1, X):
             body((x + j) % X)
 
-    def project(yy):
-        pass_mid(2 * yy + 1 - core).wait_recv()
+    def project(off):
+        yy = chip(off)
+        pass_mid(2 * yy + (core if off else 1 - core)).wait_recv()
         mid = jnp.concatenate([mid_all[2 * yy], mid_all[2 * yy + 1]], axis=1)
         part = dot(mid.T, gated).astype(BF16)
         gx_send[yy] = part.reshape(X, block, LANES)
@@ -470,18 +477,16 @@
     queue = [0]
     behind = []
     for off in order:
-        src = 2 * chip(off) + core
+        src = other_core(off)
         remote(mid_all.at[src], mid_all.at[src], mf.at[0], mr.at[src], tp=partner).wait_recv()
         pass_mid(src).start()
         ready = queue.pop(0)
-        term = project(chip(ready))
+        term = project(ready)
         act = term if act is None else act + term
         queue.append(off)
         behind.append(ready)
-        if len(behind) > 2:
-            forward_proj(chip(behind.pop(0)))
     for off in queue:
-        act = act + project(chip(off))
+        act = act + project(off)
 
     states = st[...]
     o_branch[...] = (act * states).astype(BF16)

time: 86.6 us -> 85 us (0.982)
  Pallas kernels: 85.9 us -> 84.2 us
    pallas_call x1, Pallas kernels: 84.6 us -> 82.9 us  [local(): pl.pallas_call(functools.partial(kernel, (SP, SP // Y, TP, CAP)), out_sha...]
where the time goes in v6:
time: 85 us; the launch traced here: 84.8 us
  Pallas kernels  84.2 us (99%)
    pallas_call x1, Pallas kernels, local(): pl.pallas_call(functools.partial(kernel, (SP, SP // Y, TP, CAP)), out_sha...  82.9 us

profile of v6, /device:TPU:1, one launch (start us, length us, event | category | flops | bytes accessed | tf_op | source)
XLA Modules:
  0.0 84.8 jit_solution(5538739132910908599)
XLA Ops:
  0.6 82.9 %shard_map.162 = (bf16[128,2048]{1,0:T(8,128)(2,1)S(1)}, bf16[128,2048]{1,0:T(8,128)(2,1)S(1)}, bf16[128,2048]{1,0:T(8,128)(2,1)S(1)}, f32[64,128]{1,0:T(8,128)S...) custom-call(s32[2,128]{1,0:T(2,128)} %bitcast.11, f32[2,128]{1,0:T(2,128)} %bitcast.12, ...), custom_call_target="tpu_custom_call" | custom-call | tf_op jit(solution)/shard_map/pallas_call | solution.py:590
  83.5 1.3 %shard_map.163 = (bf16[128,2048]{1,0:T(8,128)(2,1)}, bf16[128,2048]{1,0:T(8,128)(2,1)}, bf16[128,2048]{1,0:T(8,128)(2,1)}, f32[64,128]{1,0:T(8,128)}, bf16[128,1...) custom-call(bf16[128,2048]{1,0:T(8,128)(2,1)S(1)} %get-tuple-element.21.refs_0_, ...), custom_call_target="tpu_custom_call" | custom-call | tf_op jit(solution)/shard_map/pallas_call | solution.py:654
